TPU v7x, 32 devices: a whole 2x2x4 slice. The times are simulated.
32 devices in a mesh: sp: 16 (over z, y, x), tp: 2 (over core).
Axes of the slice: x: 2, y: 2, z: 4, core: 2. Of those that a mesh axis runs over, the one named last changes fastest.
Arguments:
- x_rows: bfloat16 [2048, 2048], P('sp'), may hold values from -6 to 6
- queries: bfloat16 [2048, 1024], P('sp', 'tp'), may hold values from -8 to 8
- keys: bfloat16 [2048, 512], P('sp', 'tp'), may hold values from -8 to 8
- values: bfloat16 [2048, 512], P('sp', 'tp'), may hold values from -6 to 6
- query_norm_gain: float32 [64], replicated, may hold values from 1 to 8
- key_norm_gain: float32 [64], replicated, may hold values from 1 to 8
- out_weight: bfloat16 [1024, 2048], P('tp'), may hold values from -0.1875 to 0.1875
- ffn_gain: float32 [2048], replicated, may hold values from 0.1 to 1.9
- gate_weight: bfloat16 [2048, 5120], P('sp', 'tp'), may hold values from -0.125 to 0.125
- value_weight: bfloat16 [2048, 5120], P('sp', 'tp'), may hold values from -0.125 to 0.125
- conv_gate: float32 [3, 5120], P(None, 'tp'), may hold values from -3.5 to 3.5
- conv_value: float32 [3, 5120], P(None, 'tp'), may hold values from -3.5 to 3.5
- down_weight: bfloat16 [2048, 5120], P('sp', 'tp'), may hold values from -0.078125 to 0.078125
Outputs:
- layer_out: bfloat16 [2048, 2048], P('sp')
All inputs are finite; a program needn't handle non-finite values.
Results may differ from a plain program's by a relative error of at most 0.017.
Values may be sent and summed in bfloat16 or wider, within the bound.
A program may use at most 64 MiB of HBM per device.

v0:
```python
import math

import jax
import jax.numpy as jnp
from jax import lax
from jax.sharding import PartitionSpec as P

HEAD_SIZE = 64
GRID_ROW_WIDTH = 64


eps_norm = 1e-06
theta = 10000.0


def with_halo(cells, sides, width):
    for axis, dim in sides:
        count = lax.axis_size(axis)
        ends = count - 1
        head = lax.slice_in_dim(cells, 0, width, axis=dim)
        tail = lax.slice_in_dim(cells, cells.shape[dim] - width, cells.shape[dim], axis=dim)
        cells = jnp.concatenate(
            [
                lax.ppermute(tail, axis, [(i, (i + 1) % count) for i in range(ends)]),
                cells,
                lax.ppermute(head, axis, [((i + 1) % count, i) for i in range(ends)]),
            ],
            axis=dim,
        )
    return cells


def per_head_norm(head_block, gain_vec):
    wide_vals = head_block.astype(jnp.float32)
    inverse_rms = lax.rsqrt(jnp.mean(wide_vals * wide_vals, axis=-1, keepdims=True) + eps_norm)
    return wide_vals * inverse_rms * gain_vec


def turn_half(half_vec, places):
    quarter_len = half_vec.shape[-1] // 2
    inverse_rates = 1.0 / theta ** (
        jnp.arange(quarter_len, dtype=jnp.float32) * 2.0 / half_vec.shape[-1]
    )
    angles = places.astype(jnp.float32)[:, None] * inverse_rates[None, :]
    angles = jnp.concatenate([angles, angles], axis=-1)[:, None, :]
    front_part = half_vec[..., :quarter_len]
    back_part = half_vec[..., quarter_len:]
    return half_vec * jnp.cos(angles) + jnp.concatenate(
        [-back_part, front_part], axis=-1
    ) * jnp.sin(angles)


def apply_rotary(normed_heads, token_positions):
    half_point = normed_heads.shape[-1] // 2
    grid_row = token_positions // GRID_ROW_WIDTH
    grid_col = token_positions % GRID_ROW_WIDTH
    return jnp.concatenate(
        [
            turn_half(normed_heads[..., :half_point], grid_row),
            turn_half(normed_heads[..., half_point:], grid_col),
        ],
        axis=-1,
    )


def row_norm(rows_wide, gain_vec):
    inverse_rms = lax.rsqrt(jnp.mean(rows_wide * rows_wide, axis=-1, keepdims=True) + eps_norm)
    return (rows_wide * inverse_rms * gain_vec).astype(jnp.bfloat16)


def contract_units(left_rows, right_rows):
    return lax.dot_general(
        left_rows, right_rows, (((1,), (1,)), ((), ())), preferred_element_type=jnp.float32
    )


def shards(
    x_rows,
    queries,
    keys,
    values,
    query_norm_gain,
    key_norm_gain,
    out_weight,
    ffn_gain,
    gate_weight,
    value_weight,
    conv_gate,
    conv_value,
    down_weight,
):
    collected = (
        lax.all_gather(gate_weight, "sp", axis=0, tiled=True),
        lax.all_gather(value_weight, "sp", axis=0, tiled=True),
        lax.all_gather(down_weight, "sp", axis=0, tiled=True),
    )
    tokens_here = queries.shape[0]
    query_heads = queries.shape[1] // HEAD_SIZE
    key_heads = keys.shape[1] // HEAD_SIZE
    group_width = query_heads // key_heads
    lane_rows = group_width * tokens_here
    token_positions = lax.axis_index("sp") * tokens_here + jnp.arange(tokens_here, dtype=jnp.int32)
    rotated_queries = apply_rotary(
        per_head_norm(queries.reshape(tokens_here, query_heads, HEAD_SIZE), query_norm_gain),
        token_positions,
    )
    query_lanes = rotated_queries.reshape(tokens_here, key_heads, group_width, HEAD_SIZE).transpose(
        1, 2, 0, 3
    )
    query_lanes = query_lanes.reshape(key_heads, lane_rows, HEAD_SIZE) * HEAD_SIZE ** (-0.5)
    start_state = (
        jnp.full((key_heads, lane_rows), -1e30, jnp.float32),
        jnp.zeros((key_heads, lane_rows), jnp.float32),
        jnp.zeros((key_heads, lane_rows, HEAD_SIZE), jnp.float32),
    )
    key_piece = lax.all_gather(keys, "sp", axis=0, tiled=True)
    value_piece = lax.all_gather(values, "sp", axis=0, tiled=True)
    row_count = key_piece.shape[0]
    key_places = jnp.arange(row_count, dtype=jnp.int32)
    turned = apply_rotary(
        per_head_norm(key_piece.reshape(row_count, key_heads, HEAD_SIZE), key_norm_gain), key_places
    )
    key_span = math.gcd(row_count, 2048)
    span_count = row_count // key_span
    turned = turned.reshape(span_count, key_span, key_heads, HEAD_SIZE)
    value_matrix = value_piece.reshape(span_count, key_span, key_heads, HEAD_SIZE)

    def one_span(state_now, inputs):
        running_top, denominator, weighted = state_now
        key_block, value_block = inputs
        scores = jnp.einsum("hrd,shd->hrs", query_lanes, key_block, precision=lax.Precision.HIGHEST)
        new_top = jnp.maximum(running_top, jnp.max(scores, axis=-1))
        factor = jnp.exp(running_top - new_top)
        weights = jnp.exp(scores - new_top[..., None])
        denominator = denominator * factor + jnp.sum(weights, axis=-1)
        weighted = weighted * factor[..., None] + jnp.einsum(
            "hrs,shd->hrd",
            weights.astype(jnp.bfloat16),
            value_block,
            preferred_element_type=jnp.float32,
        )
        return ((new_top, denominator, weighted), None)

    folded_state, _ = lax.scan(one_span, start_state, (turned, value_matrix))
    running_top, denominator, weighted = folded_state
    attended = (weighted / denominator[..., None]).reshape(
        key_heads, group_width, tokens_here, HEAD_SIZE
    )
    attended = (
        attended.transpose(2, 0, 1, 3)
        .reshape(tokens_here, query_heads * HEAD_SIZE)
        .astype(jnp.bfloat16)
    )
    share_rows = tokens_here // lax.axis_size("tp")
    head_share = lax.psum_scatter(
        jnp.dot(attended, out_weight, preferred_element_type=jnp.float32).astype(jnp.bfloat16),
        "tp",
        scatter_dimension=0,
        tiled=True,
    ).astype(jnp.float32)
    own_rows = lax.dynamic_slice_in_dim(x_rows, lax.axis_index("tp") * share_rows, share_rows, 0)
    middle_rows = own_rows.astype(jnp.float32) + head_share
    normed = lax.all_gather(row_norm(middle_rows, ffn_gain), "tp", axis=0, tiled=True)
    unit_local = gate_weight.shape[1]
    gate_pre = jnp.dot(normed, collected[0], preferred_element_type=jnp.float32).astype(
        jnp.bfloat16
    )
    value_pre = jnp.dot(normed, collected[1], preferred_element_type=jnp.float32).astype(
        jnp.bfloat16
    )
    joined = jnp.concatenate([gate_pre, value_pre], axis=1)
    padded = with_halo(joined, (("sp", 0),), 1).astype(jnp.float32)
    conv_taps = jnp.concatenate([conv_gate, conv_value], axis=1)
    convolved = conv_taps[0] * padded[:-2] + conv_taps[1] * padded[1:-1] + conv_taps[2] * padded[2:]
    hidden = (jax.nn.silu(convolved[:, :unit_local]) * convolved[:, unit_local:]).astype(
        jnp.bfloat16
    )
    unit_share = lax.psum_scatter(
        contract_units(hidden, collected[2]).astype(jnp.bfloat16),
        "tp",
        scatter_dimension=0,
        tiled=True,
    ).astype(jnp.float32)
    finished = (middle_rows + unit_share).astype(jnp.bfloat16)
    return lax.all_gather(finished, "tp", axis=0, tiled=True)


def solution(mesh):
    placed = (
        P("sp", None),
        P("sp", "tp"),
        P("sp", "tp"),
        P("sp", "tp"),
        P(),
        P(),
        P("tp", None),
        P(),
        P("sp", "tp"),
        P("sp", "tp"),
        P(None, "tp"),
        P(None, "tp"),
        P("sp", "tp"),
    )
    return jax.shard_map(
        shards, mesh=mesh, in_specs=placed, out_specs=P("sp", None), check_vma=False
    )
```

profile of v0, /device:TPU:7, one launch (start us, length us, event | category | flops | bytes accessed | tf_op | source)
XLA Modules:
  0.0 564.6 jit_solution(3756514513751878015)
XLA Ops:
  6.5 0.7 all-gather.6.cloned.1.call-update
  7.3 0.7 all-gather.8.cloned.1.call-update
  8.0 0.0 reduce-scatter.3.cloned.1.call-start
  8.1 0.1 broadcast_multiply_fusion.3
  8.2 0.1 fusion.39
  8.2 0.1 fusion.41
  8.3 1.0 copy.16
  9.4 0.7 fusion.29
  10.2 0.1 broadcast_multiply_fusion.1
  10.3 1.9 fusion.33
  12.2 51.3 %all-gather.6.cloned.1.call-done = bf16[2048,256]{1,0:T(8,128)(2,1)} async-done(((bf16[128,256]{1,0:T(8,128)(2,1)}), bf16[2048,256]{1,0:T(8,128)(2,1)}) %all-gather.6.cloned.1.call-update) | async-done | bytes 1048592 | tf_op jit(solution)/shard_map/all_gather | solution.py:116
  63.5 2.6 copy.18
  66.1 2.0 multiply_reduce_fusion
  68.1 0.2 copy-done.3
  68.3 0.4 multiply_multiply_fusion
  68.7 0.2 slice_negate_fusion.1
  69.0 0.5 fusion.25
  69.5 7.3 %fusion.57 = (f32[4,256]{1,0:T(4,128)S(1)}, f32[4,256,2048]{2,1,0:T(8,128)S(1)}) fusion(f32[2048,4,32]{0,2,1:T(8,128)S(1)} %get-tuple-element.18, f32[2048,4,32]{0,2,1:T(8,128)S(1)} %get-tuple-element.17, f32[4,2,8,8,128]{4,3,2,1,0:T(8,128)S(1)} %bitcast.37), kind=kOutput, calls=%fused_computation.107 | convolution fusion | flops 1613233152 | bytes 10752000 | tf_op jit(solution)/shard_map/while/body/eval_jaxpr/hrd,shd->hrs/dot_general | solution.py:131
  76.8 1.3 fusion
  78.2 2.0 copy-done.2
  80.1 40.1 %all-gather.8.cloned.1.call-done = bf16[2048,256]{1,0:T(8,128)(2,1)} async-done(((bf16[128,256]{1,0:T(8,128)(2,1)}), bf16[2048,256]{1,0:T(8,128)(2,1)}) %all-gather.8.cloned.1.call-update) | async-done | bytes 1048592 | tf_op jit(solution)/shard_map/all_gather | solution.py:117
  120.2 1.7 copy.19
  121.9 4.9 fusion.21
  126.9 1.3 convolution_convert_fusion.2
  128.1 0.0 all-gather.12.cloned.1.call-start
  128.2 0.5 all-gather.12.cloned.1.call-update
  128.8 0.5 all-gather.10.cloned.1.call-update
  129.4 0.5 all-gather.14.cloned.1.call-update
  129.9 0.0 reduce-scatter.5.cloned.1.call-start
  130.0 8.7 %reduce-scatter.3.cloned.1.call-done = bf16[64,2048]{1,0:T(8,128)(2,1)} async-done(((bf16[128,2048]{1,0:T(8,128)(2,1)}), bf16[64,2048]{1,0:T(8,128)(2,1)}) %reduce-scatter.3.cloned.1.call-update) | async-done | bytes 262160 | tf_op jit(solution)/shard_map/reduce_scatter | solution.py:155
  138.7 1.1 multiply_reduce_fusion.1
  139.8 1.1 multiply_convert_fusion
  140.9 2.2 all_gather.23
  143.1 128.0 %all-gather.12.cloned.1.call-done = bf16[2048,2560]{1,0:T(8,128)(2,1)} async-done(((bf16[128,2560]{1,0:T(8,128)(2,1)}), bf16[2048,2560]{1,0:T(8,128)(2,1)}) %all-gather.12.cloned.1.call-update) | async-done | bytes 10485776 | tf_op jit(solution)/shard_map/all_gather | solution.py:94
  271.1 5.5 convolution_convert_fusion
  276.6 126.7 %all-gather.10.cloned.1.call-done = bf16[2048,2560]{1,0:T(8,128)(2,1)} async-done(((bf16[128,2560]{1,0:T(8,128)(2,1)}), bf16[2048,2560]{1,0:T(8,128)(2,1)}) %all-gather.10.cloned.1.call-update) | async-done | bytes 10485776 | tf_op jit(solution)/shard_map/all_gather | solution.py:93
  403.3 5.5 convolution_convert_fusion.1
  408.8 2.5 collective-permute-start
  411.4 2.8 collective-permute-start.1
  414.2 3.6 collective-permute-done.1
  417.8 0.4 maximum_convert_fusion
  418.2 2.3 fusion.5
  420.5 115.0 %all-gather.14.cloned.1.call-done = bf16[2048,2560]{1,0:T(8,128)(2,1)} async-done(((bf16[128,2560]{1,0:T(8,128)(2,1)}), bf16[2048,2560]{1,0:T(8,128)(2,1)}) %all-gather.14.cloned.1.call-update) | async-done | bytes 10485776 | tf_op jit(solution)/shard_map/all_gather | solution.py:95
  535.5 9.2 %convolution_convert_fusion.3 = bf16[128,2048]{1,0:T(8,128)(2,1)} fusion(bf16[2048,2560]{1,0:T(8,128)(2,1)} %all-gather.14.cloned.1.call-done, f32[128,5120]{1,0:T(8,128)} %fusion.5), kind=kOutput, calls=%fused_computation.13 | convolution fusion | flops 1344405504 | bytes 13631488 | tf_op jit(solution)/shard_map/dot_general | solution.py:72
  544.7 9.0 %reduce-scatter.5.cloned.1.call-done = bf16[64,2048]{1,0:T(8,128)(2,1)} async-done(((bf16[128,2048]{1,0:T(8,128)(2,1)}), bf16[64,2048]{1,0:T(8,128)(2,1)}) %reduce-scatter.5.cloned.1.call-update) | async-done | bytes 262160 | tf_op jit(solution)/shard_map/reduce_scatter | solution.py:178
  553.8 1.0 add_convert_fusion
  554.8 2.2 all_gather.27
  557.0 0.8 copy.33
  (43 shorter events, 0.5 us)
Async XLA Ops:
  6.5 120.3 %copy-start = (bf16[512,2048]{1,0:T(8,128)(2,1)S(1)}, bf16[512,2048]{1,0:T(8,128)(2,1)}, u32[]{:S(2)}) copy-start(bf16[512,2048]{1,0:T(8,128)(2,1)} %param.19) | copy-start | bytes 6291460
  6.5 57.0 %all-gather.6.cloned.1.call-start = ((), (), s32[]{:S(2)}) async-start(), calls=%async_computation.2 | async-start | bytes 1114112 | tf_op jit(solution)/shard_map/all_gather | solution.py:116
  7.3 113.0 %all-gather.8.cloned.1.call-start = ((), (), s32[]{:S(2)}) async-start(), calls=%async_computation.3 | async-start | bytes 1114112 | tf_op jit(solution)/shard_map/all_gather | solution.py:117
  8.0 130.7 %reduce-scatter.3.cloned.1.call-start = ((), (), s32[]{:S(2)}) async-start(), calls=%async_computation.4 | async-start | bytes 786432 | tf_op jit(solution)/shard_map/reduce_scatter | solution.py:155
  12.2 55.9 %copy-start.9 = (f32[64]{0:T(128)S(1)}, f32[64]{0:T(128)}, u32[]{:S(2)}) copy-start(f32[64]{0:T(128)} %param.18) | copy-start | bytes 772
  66.1 2.2 copy-start.3
  76.8 3.3 copy-start.2
  126.8 3.1 copy-start.6
  126.8 3.2 copy-start.7
  126.8 11.8 %copy-start.5 = (bf16[128,2048]{1,0:T(8,128)(2,1)S(1)}, bf16[128,2048]{1,0:T(8,128)(2,1)}, u32[]{:S(2)}) copy-start(bf16[128,2048]{1,0:T(8,128)(2,1)} %param.13) | copy-start | bytes 1572868
  126.8 13.0 %copy-start.8 = (f32[2048]{0:T(1024)S(1)}, f32[2048]{0:T(1024)}, u32[]{:S(2)}) copy-start(f32[2048]{0:T(1024)} %param.20) | copy-start | bytes 24580
  128.1 142.9 %all-gather.12.cloned.1.call-start = ((), (), s32[]{:S(2)}) async-start(), calls=%async_computation.6 | async-start | bytes 11141120 | tf_op jit(solution)/shard_map/all_gather | solution.py:94
  128.7 274.5 %all-gather.10.cloned.1.call-start = ((), (), s32[]{:S(2)}) async-start(), calls=%async_computation.5 | async-start | bytes 11141120 | tf_op jit(solution)/shard_map/all_gather | solution.py:93
  129.3 406.2 %all-gather.14.cloned.1.call-start = ((), (), s32[]{:S(2)}) async-start(), calls=%async_computation.7 | async-start | bytes 11141120 | tf_op jit(solution)/shard_map/all_gather | solution.py:95
  129.9 423.9 %reduce-scatter.5.cloned.1.call-start = ((), (), s32[]{:S(2)}) async-start(), calls=%async_computation.8 | async-start | bytes 786432 | tf_op jit(solution)/shard_map/reduce_scatter | solution.py:178
  408.8 5.4 collective-permute-start
  411.4 6.4 %collective-permute-start.1 = (bf16[1,5120]{1,0:T(2,128)(2,1)S(1)}, bf16[1,5120]{1,0:T(2,128)(2,1)S(1)}, u32[]{:S(2)}, u32[]{:S(2)}) collective-permute-start(bf16[1,5120]{1,0:T(2,128)(2,1)S(1)} %get-tuple-element.33), channel_id=1, source_target_pairs={{2,0},{4,2},{6,4},{8,6},{10,8},{12,10},{14,12},{16,14},{18,16},{20... | collective-permute-start | bytes 30728 | tf_op jit(solution)/shard_map/ppermute | solution.py:26
  420.5 133.2 %copy-start.4 = (bf16[64,2048]{1,0:T(8,128)(2,1)S(1)}, bf16[64,2048]{1,0:T(8,128)(2,1)}, u32[]{:S(2)}) copy-start(bf16[64,2048]{1,0:T(8,128)(2,1)} %reduce-scatter.3.cloned.1.call-done) | copy-start | bytes 786436
  535.5 22.3 %copy-start.1 = (bf16[512,2048]{1,0:T(8,128)(2,1)S(1)}, bf16[512,2048]{1,0:T(8,128)(2,1)}, u32[]{:S(2)}) copy-start(bf16[512,2048]{1,0:T(8,128)(2,1)} %param.19) | copy-start | bytes 6291460
Sparse Core Ops, SparseCore 0:
  10.1 53.3 all-gather.5
  66.3 53.9 all-gather.7
  128.3 10.3 reduce-scatter.2
  141.2 129.8 all-gather.11
  273.6 129.6 all-gather.9
  405.8 129.6 all-gather.13
  544.8 8.8 reduce-scatter.4
where the time goes:
time: 566 us; the launch traced here: 565 us
  waiting for transfers between devices  485 us (86%)
  matrix products  33.7 us (6%)
  between operations  13.8 us (2%)
  other arithmetic  13.5 us (2%)
  local copies, waits for them, and re-layouts  8.36 us (1%)
    all_gather x1, waiting for transfers between devices, shards(): lax.all_gather(value_weight, 'sp', axis=0, tiled=True)  128 us
    all_gather x1, waiting for transfers between devices, shards(): lax.all_gather(gate_weight, 'sp', axis=0, tiled=True)  127 us
    all_gather x1, waiting for transfers between devices, shards(): lax.all_gather(down_weight, 'sp', axis=0, tiled=True)  115 us
    all_gather x1, waiting for transfers between devices, shards(): key_piece = lax.all_gather(keys, 'sp', axis=0, tiled=True)  51.3 us
    all_gather x1, waiting for transfers between devices, shards(): value_piece = lax.all_gather(values, 'sp', axis=0, tiled=True)  40.1 us
  transfers between devices with their start and end apart: 9, of which 8 were waited for; matrix products, arithmetic and copies ran while one was open for 6% of the time, Pallas kernels for 0%

commit v1 on v0

--- a/solution.py
+++ b/solution.py
@@ -1,8 +1,11 @@
+import functools
 import math
 
 import jax
 import jax.numpy as jnp
 from jax import lax
+from jax.experimental import pallas as pl
+from jax.experimental.pallas import tpu as pltpu
 from jax.sharding import PartitionSpec as P
 
 HEAD_SIZE = 64
@@ -184,6 +187,471 @@
     finished = (middle_rows + unit_share).astype(jnp.bfloat16)
     return lax.all_gather(finished, "tp", axis=0, tiled=True)
 
+LANES = 128
+MESH = pl.DeviceIdType.MESH
+BF = jnp.bfloat16
+F32 = jnp.float32
+
+
+def nt(left, right):
+    return lax.dot_general(left, right, (((1,), (1,)), ((), ())), preferred_element_type=F32)
+
+
+def layer_kernel(
+    n, halves, x_ref, q_ref, kv_ref, qg_ref, kg_ref, cos_ref, sin_ref, wo_ref, fg_ref, w_ref,
+    cg_ref, cv_ref, out_ref,
+    kvbuf, qbuf, kcat, qcat, att_s, attbuf, po_s, po_r, mid, allnorm, halo_s, halo_r, wrecv,
+    pre_g, pre_v, part, ddbuf, own_sum, rs_s, rs_r, fin_s, fin_r,
+    loc, kv_ss, kv_rs, q_ss, q_rs, w_ss, w_rs, o_ss, o_rs, po_sem, ag_ss, ag_rs, fw_ss, fw_rs,
+    h_ss, h_rs, dd_ss, dd_rs, c_ss, c_rs, fin_sem,
+):
+    sp = lax.axis_index("sp")
+    core = lax.axis_index("tp")
+    mate = 1 - core
+    rows = x_ref.shape[0]
+    half_rows = rows // 2
+    width = x_ref.shape[1]
+    kv_heads = kv_ref.shape[1] // LANES
+    group = n // halves
+    tokens = n * rows
+    q_tokens = kv_heads * rows
+    units = w_ref.shape[1] // 3
+    head_at = lax.rem(sp, kv_heads)
+    q_base = sp - head_at
+    in_group = lax.rem(sp, group)
+    g_base = sp - in_group
+    half_at = sp // group
+
+    def remote(src, dst, ss, rs, device):
+        return pltpu.make_async_remote_copy(
+            src_ref=src, dst_ref=dst, send_sem=ss, recv_sem=rs, device_id=device, device_id_type=MESH
+        )
+
+    def lane_block(k):
+        return pl.ds(pl.multiple_of(k * LANES, LANES), LANES)
+
+    def span(start, size, unit):
+        return pl.ds(pl.multiple_of(start, unit), size)
+
+    def loop(lo, hi, fn):
+        def step(k, carry):
+            fn(k)
+            return carry
+
+        lax.fori_loop(lo, hi, step, 0)
+
+    barrier = pltpu.get_barrier_semaphore()
+
+    def greet(d):
+        t = lax.rem(sp + d, n)
+        pl.semaphore_signal(barrier, inc=1, device_id=(t, core), device_id_type=MESH)
+        pl.semaphore_signal(barrier, inc=1, device_id=(t, mate), device_id_type=MESH)
+
+    loop(1, n, greet)
+    pl.semaphore_signal(barrier, inc=1, device_id=(sp, mate), device_id_type=MESH)
+    pl.semaphore_wait(barrier, 2 * n - 1)
+
+    def q_copy(d):
+        t = q_base + lax.rem(head_at + d, kv_heads)
+        return remote(
+            q_ref.at[:, lane_block(t - q_base)], qbuf.at[span(head_at * rows, rows, rows)],
+            q_ss.at[d], q_rs.at[d], (t, core),
+        )
+
+    def kv_copy(d):
+        t = lax.rem(sp + d, n)
+        return remote(
+            kv_ref.at[:, lane_block(lax.rem(t, kv_heads))], kvbuf.at[span(sp * rows, rows, rows)],
+            kv_ss.at[d], kv_rs.at[d], (t, core),
+        )
+
+    def w_copy(d):
+        t = lax.rem(sp + d, n)
+        return remote(
+            w_ref.at[lax.rem(t, group)], wrecv.at[:, lane_block(sp)],
+            w_ss.at[d], w_rs.at[d], (t, core),
+        )
+
+    own_q = pltpu.make_async_copy(
+        q_ref.at[:, lane_block(head_at)], qbuf.at[span(head_at * rows, rows, rows)], loc.at[0]
+    )
+    own_kv = pltpu.make_async_copy(
+        kv_ref.at[:, lane_block(head_at)], kvbuf.at[span(sp * rows, rows, rows)], loc.at[1]
+    )
+    own_w = pltpu.make_async_copy(w_ref.at[in_group], wrecv.at[:, lane_block(sp)], loc.at[2])
+    own_q.start()
+    own_kv.start()
+    loop(1, kv_heads, lambda d: q_copy(d).start())
+    loop(1, n, lambda d: kv_copy(d).start())
+    loop(1, n, lambda d: w_copy(d).start())
+    own_w.start()
+
+    lane = lax.broadcasted_iota(jnp.int32, (GRID_ROW_WIDTH, LANES), 1)
+    low = lane < HEAD_SIZE
+    first = lax.rem(lane, 2 * HEAD_SIZE // 4) < HEAD_SIZE // 4
+    by_row = lax.rem(lane, HEAD_SIZE) < HEAD_SIZE // 2
+
+    def turn(vals, grid_row):
+        cos = jnp.where(by_row, cos_ref[pl.ds(grid_row, 1), :], cos_ref[:GRID_ROW_WIDTH, :])
+        sin = jnp.where(by_row, sin_ref[pl.ds(grid_row, 1), :], sin_ref[:GRID_ROW_WIDTH, :])
+        quarter = HEAD_SIZE // 4
+        swapped = jnp.where(
+            first, pltpu.roll(vals, LANES - quarter, 1), pltpu.roll(vals, quarter, 1)
+        )
+        return vals * cos + swapped * sin
+
+    def split(vals):
+        top = vals.astype(BF).astype(F32)
+        return top, (vals - top).astype(BF).astype(F32)
+
+    own_q.wait()
+
+    def q_wait(d):
+        s = lax.rem(head_at + kv_heads - d, kv_heads)
+        dst = qbuf.at[span(s * rows, rows, rows)]
+        remote(dst, dst, q_ss.at[d], q_rs.at[d], (q_base + s, core)).wait_recv()
+
+    loop(1, kv_heads, q_wait)
+
+    def make_q(r):
+        at = span(r * GRID_ROW_WIDTH, GRID_ROW_WIDTH, GRID_ROW_WIDTH)
+        vals = qbuf[at, :].astype(F32)
+        sq = vals * vals
+        low_sum = jnp.sum(jnp.where(low, sq, 0.0), axis=1, keepdims=True)
+        high_sum = jnp.sum(jnp.where(low, 0.0, sq), axis=1, keepdims=True)
+        inverse = jnp.where(
+            low,
+            lax.rsqrt(low_sum * (1.0 / HEAD_SIZE) + eps_norm),
+            lax.rsqrt(high_sum * (1.0 / HEAD_SIZE) + eps_norm),
+        )
+        turned = turn(vals * inverse * qg_ref[...], q_base * (rows // GRID_ROW_WIDTH) + r)
+        top, rest = split(turned * HEAD_SIZE ** (-0.5))
+        qcat[at, :] = jnp.where(low, top, pltpu.roll(rest, HEAD_SIZE, 1)).astype(BF)
+        later = span(q_tokens + r * GRID_ROW_WIDTH, GRID_ROW_WIDTH, GRID_ROW_WIDTH)
+        qcat[later, :] = jnp.where(low, pltpu.roll(top, HEAD_SIZE, 1), rest).astype(BF)
+
+    loop(0, q_tokens // GRID_ROW_WIDTH, make_q)
+    own_kv.wait()
+
+    def kv_wait(d):
+        s = lax.rem(sp + n - d, n)
+        dst = kvbuf.at[span(s * rows, rows, rows)]
+        remote(dst, dst, kv_ss.at[d], kv_rs.at[d], (s, core)).wait_recv()
+
+    loop(1, n, kv_wait)
+
+    def make_k(r):
+        at = span(r * GRID_ROW_WIDTH, GRID_ROW_WIDTH, GRID_ROW_WIDTH)
+        vals = kvbuf[at, :].astype(F32)
+        total = jnp.sum(jnp.where(low, vals * vals, 0.0), axis=1, keepdims=True)
+        turned = turn(
+            vals * lax.rsqrt(total * (1.0 / HEAD_SIZE) + eps_norm) * kg_ref[...], r
+        )
+        top, rest = split(turned)
+        kcat[at, :LANES] = jnp.where(low, top, pltpu.roll(top, HEAD_SIZE, 1)).astype(BF)
+        kcat[at, LANES:] = jnp.where(low, rest, pltpu.roll(rest, HEAD_SIZE, 1)).astype(BF)
+
+    loop(0, tokens // GRID_ROW_WIDTH, make_k)
+
+    def o_copy(d):
+        k = lax.rem(head_at + d, kv_heads)
+        return remote(
+            att_s.at[span(k * rows, rows, rows)], attbuf.at[:, lane_block(head_at)],
+            o_ss.at[d], o_rs.at[d], (q_base + k, core),
+        )
+
+    low_rows = lax.broadcasted_iota(jnp.int32, (rows, LANES), 1) < HEAD_SIZE
+
+    def attend(k):
+        both = jnp.concatenate(
+            [qcat[span(k * rows, rows, rows), :], qcat[span(q_tokens + k * rows, rows, rows), :]],
+            axis=0,
+        )
+        scores = nt(jnp.concatenate([both, both], axis=1), kcat[...])
+        shifted = jnp.exp(scores - jnp.max(scores, axis=1, keepdims=True))
+        total = jnp.sum(shifted, axis=1, keepdims=True)
+        summed = jnp.dot(shifted.astype(BF), kvbuf[...], preferred_element_type=F32) / total
+        return jnp.where(
+            low_rows, pltpu.roll(summed[:rows], HEAD_SIZE, 1), summed[rows:]
+        ).astype(BF)
+
+    def attend_send(d):
+        k = lax.rem(head_at + d, kv_heads)
+        att_s[span(k * rows, rows, rows), :] = attend(k)
+
+        @pl.when(d < kv_heads)
+        def _():
+            o_copy(d).start()
+
+    loop(1, kv_heads + 1, attend_send)
+    attbuf[:, lane_block(head_at)] = att_s[span(head_at * rows, rows, rows), :]
+
+    def o_wait(d):
+        s = lax.rem(head_at + kv_heads - d, kv_heads)
+        dst = attbuf.at[:, lane_block(s)]
+        remote(dst, dst, o_ss.at[d], o_rs.at[d], (q_base + s, core)).wait_recv()
+
+    loop(1, kv_heads, o_wait)
+
+    po_s[...] = jnp.dot(attbuf[...], wo_ref[...], preferred_element_type=F32).astype(BF)
+    po_copy = remote(
+        po_s.at[span(mate * half_rows, half_rows, half_rows)], po_r, po_sem.at[0], po_sem.at[1],
+        (sp, mate),
+    )
+    po_copy.start()
+    mine = span(core * half_rows, half_rows, half_rows)
+    base = x_ref[mine, :].astype(F32) + po_s[mine, :].astype(F32)
+    po_copy.wait_recv()
+    middle = base + po_r[...].astype(F32)
+    mid[...] = middle
+    scaled = lax.rsqrt(jnp.mean(middle * middle, axis=1, keepdims=True) + eps_norm)
+    normed = (middle * scaled * fg_ref[...]).astype(BF)
+
+    def slot(k, c):
+        return allnorm.at[span(k * rows + c * half_rows, half_rows, half_rows)]
+
+    allnorm[span(in_group * rows + core * half_rows, half_rows, half_rows), :] = normed
+
+    wide = normed.astype(F32)
+    pieces = width // LANES
+
+    def halo_fill(row):
+        for k in range(pieces):
+            halo_s[k : k + 1, :] = wide[row : row + 1, k * LANES : (k + 1) * LANES]
+
+    def halo_copy(k):
+        other = (1 - half_at) * group
+        return remote(
+            halo_s, halo_r, h_ss.at[k], h_rs.at[0], (other + k // 2, lax.rem(k, 2))
+        )
+
+    sends_first = jnp.logical_and(jnp.logical_and(half_at == 1, in_group == 0), core == 0)
+    sends_last = jnp.logical_and(jnp.logical_and(half_at == 0, in_group == group - 1), core == 1)
+
+    @pl.when(sends_first)
+    def _():
+        halo_fill(0)
+
+    @pl.when(sends_last)
+    def _():
+        halo_fill(half_rows - 1)
+
+    sends = jnp.logical_or(sends_first, sends_last)
+
+    @pl.when(sends)
+    def _():
+        loop(0, 2 * group, lambda k: halo_copy(k).start())
+
+    def ag_copy(d):
+        t = g_base + lax.rem(in_group + d, group)
+        return remote(
+            slot(in_group, core), slot(in_group, core), ag_ss.at[d], ag_rs.at[d], (t, core)
+        )
+
+    def fw_copy(d):
+        s = lax.rem(in_group + group - d, group)
+        return remote(slot(s, core), slot(s, core), fw_ss.at[d], fw_rs.at[d], (sp, mate))
+
+    loop(1, group, lambda d: ag_copy(d).start())
+    fw_copy(0).start()
+
+    def ag_wait(d):
+        s = lax.rem(in_group + group - d, group)
+        remote(slot(s, core), slot(s, core), ag_ss.at[d], ag_rs.at[d], (sp, mate)).wait_recv()
+        fw_copy(d).start()
+
+    own_w.wait()
+
+    def w_wait(d):
+        s = lax.rem(sp + n - d, n)
+        dst = wrecv.at[:, lane_block(s)]
+        remote(dst, dst, w_ss.at[d], w_rs.at[d], (s, core)).wait_recv()
+
+    loop(1, n, w_wait)
+
+    def up(block):
+        both = nt(block, wrecv[: 2 * units, :]).astype(BF).astype(F32)
+        return both[:, :units], both[:, units:]
+
+    def up_rows(d):
+        s = lax.rem(in_group + group - d, group)
+
+        @pl.when(d > 0)
+        def _():
+            ag_wait(d)
+
+        remote(slot(s, mate), slot(s, mate), fw_ss.at[d], fw_rs.at[d], (sp, mate)).wait_recv()
+        gate, value = up(allnorm[span(s * rows, rows, rows), :])
+        at = span(8 + s * rows, rows, 8)
+        pre_g[at, :] = gate
+        pre_v[at, :] = value
+
+    loop(0, group, up_rows)
+    remote(halo_r, halo_r, h_ss.at[0], h_rs.at[0], (sp, mate)).wait_recv()
+    edge = jnp.concatenate([halo_r[k : k + 1, :] for k in range(pieces)], axis=1)
+    gate, value = up(jnp.broadcast_to(edge, (16, width)).astype(BF))
+    span_rows = group * rows
+    zeros = jnp.zeros((8, units), F32)
+    pre_g[:8, :] = jnp.where(half_at == 1, gate[:8], zeros)
+    pre_v[:8, :] = jnp.where(half_at == 1, value[:8], zeros)
+    pre_g[8 + span_rows :, :] = jnp.where(half_at == 0, gate[:8], zeros)
+    pre_v[8 + span_rows :, :] = jnp.where(half_at == 0, value[:8], zeros)
+
+    def convolve(ref, taps, k):
+        block = ref[span(k * rows, rows + 16, 8), :]
+        return (
+            taps[0:1, :] * block[7 : 7 + rows]
+            + taps[1:2, :] * block[8 : 8 + rows]
+            + taps[2:3, :] * block[9 : 9 + rows]
+        )
+
+    def dd_copy(d):
+        return remote(
+            part.at[d, span(mate * half_rows, half_rows, half_rows)], ddbuf.at[d],
+            dd_ss.at[d], dd_rs.at[d], (sp, mate),
+        )
+
+    def c_copy(d):
+        t = g_base + lax.rem(in_group + d, group)
+        return remote(rs_s.at[d], rs_r.at[d], c_ss.at[d], c_rs.at[d], (t, core))
+
+    def combine(d):
+        dd_copy(d).wait_recv()
+        return part[d, mine, :].astype(F32) + ddbuf[d].astype(F32)
+
+    def send_sum(d):
+        rs_s[d] = combine(d).astype(BF)
+        c_copy(d).start()
+
+    def down(d):
+        k = lax.rem(in_group + d, group)
+        gate = convolve(pre_g, cg_ref, k)
+        value = convolve(pre_v, cv_ref, k)
+        hidden = (gate / (1.0 + jnp.exp(-gate)) * value).astype(BF)
+        e = lax.rem(d, group)
+        part[e] = jnp.dot(hidden, wrecv[2 * units :, :], preferred_element_type=F32).astype(BF)
+        dd_copy(e).start()
+
+        @pl.when(d > 1)
+        def _():
+            send_sum(d - 1)
+
+    loop(1, group + 1, down)
+    own_sum[...] = mid[...] + combine(0)
+
+    def add_in(d):
+        remote(rs_r.at[d], rs_r.at[d], c_ss.at[d], c_rs.at[d], (sp, mate)).wait_recv()
+        own_sum[...] = own_sum[...] + rs_r[d].astype(F32)
+
+    loop(1, group, add_in)
+    fin_s[...] = own_sum[...].astype(BF)
+    fin_copy = remote(fin_s, fin_r, fin_sem.at[0], fin_sem.at[1], (sp, mate))
+    fin_copy.start()
+    out_ref[mine, :] = fin_s[...]
+
+    loop(1, kv_heads, lambda d: q_copy(d).wait_send())
+    loop(1, n, lambda d: kv_copy(d).wait_send())
+    loop(1, n, lambda d: w_copy(d).wait_send())
+    loop(1, kv_heads, lambda d: o_copy(d).wait_send())
+    po_copy.wait_send()
+    loop(1, group, lambda d: ag_copy(d).wait_send())
+    loop(0, group, lambda d: fw_copy(d).wait_send())
+
+    @pl.when(sends)
+    def _():
+        loop(0, 2 * group, lambda k: halo_copy(k).wait_send())
+
+    loop(0, group, lambda d: dd_copy(d).wait_send())
+    loop(1, group, lambda d: c_copy(d).wait_send())
+    fin_copy.wait_send()
+    fin_copy.wait_recv()
+    out_ref[span(mate * half_rows, half_rows, half_rows), :] = fin_r[...]
+
+
+def rotary_tables(count):
+    lanes = jnp.arange(LANES)
+    length = HEAD_SIZE // 2
+    rate_at = (lanes % (length // 2)).astype(F32)
+    rates = 1.0 / theta ** (rate_at * 2.0 / length)
+    angles = jnp.arange(count, dtype=F32)[:, None] * rates[None, :]
+    sign = jnp.where(lanes % length < length // 2, -1.0, 1.0)
+    return jnp.cos(angles), jnp.sin(angles) * sign[None, :]
+
+
+def kernel_shards(
+    n, halves, x_rows, queries, keys, values, query_norm_gain, key_norm_gain, out_weight, ffn_gain,
+    gate_weight, value_weight, conv_gate, conv_value, down_weight,
+):
+    rows, width = x_rows.shape
+    kv_heads = keys.shape[1] // HEAD_SIZE
+    group = n // halves
+    unit_local = gate_weight.shape[1]
+    units = unit_local // group
+    depth = gate_weight.shape[0]
+    kv = jnp.concatenate(
+        [keys.reshape(rows, kv_heads, HEAD_SIZE), values.reshape(rows, kv_heads, HEAD_SIZE)], axis=-1
+    ).reshape(rows, kv_heads * LANES)
+    turned = [
+        w.T.reshape(group, units, depth) for w in (gate_weight, value_weight, down_weight)
+    ]
+    weights = jnp.concatenate(turned, axis=1)
+    chip = lax.rem(lax.axis_index("sp"), group)
+    taps = [lax.dynamic_slice_in_dim(t, chip * units, units, 1) for t in (conv_gate, conv_value)]
+    cos, sin = rotary_tables(max(GRID_ROW_WIDTH, n * rows // GRID_ROW_WIDTH))
+    tokens, q_tokens, span_rows = n * rows, kv_heads * rows, group * rows
+    half_rows = rows // 2
+    dma = pltpu.SemaphoreType.DMA
+    vm = pltpu.VMEM
+    scratch = [
+        vm((tokens, LANES), BF), vm((q_tokens, LANES), BF), vm((tokens, 2 * LANES), BF),
+        vm((2 * q_tokens, LANES), BF), vm((q_tokens, LANES), BF), vm((rows, kv_heads * LANES), BF),
+        vm((rows, width), BF), vm((half_rows, width), BF), vm((half_rows, width), F32),
+        vm((span_rows, width), BF), vm((width // LANES, LANES), F32),
+        vm((width // LANES, LANES), F32), vm((3 * units, width), BF),
+        vm((span_rows + 16, units), F32), vm((span_rows + 16, units), F32),
+        vm((group, rows, width), BF), vm((group, half_rows, width), BF),
+        vm((half_rows, width), F32), vm((group, half_rows, width), BF),
+        vm((group, half_rows, width), BF), vm((half_rows, width), BF), vm((half_rows, width), BF),
+        dma((3,)), dma((n,)), dma((n,)), dma((kv_heads,)), dma((kv_heads,)), dma((n,)), dma((n,)),
+        dma((kv_heads,)), dma((kv_heads,)), dma((2,)), dma((group,)), dma((group,)),
+        dma((group,)), dma((group,)), dma((2 * group,)), dma((1,)), dma((group,)), dma((group,)),
+        dma((group,)), dma((group,)), dma((2,)),
+    ]
+    args = (
+        x_rows, queries, kv, jnp.tile(query_norm_gain, 2)[None, :], jnp.tile(key_norm_gain, 2)[None, :],
+        cos, sin, out_weight, ffn_gain[None, :], weights, taps[0], taps[1],
+    )
+    return pl.pallas_call(
+        lambda *refs: layer_kernel(n, halves, *refs),
+        out_shape=jax.ShapeDtypeStruct((rows, width), BF),
+        in_specs=[pl.BlockSpec(memory_space=pltpu.VMEM)] * len(args),
+        out_specs=pl.BlockSpec(memory_space=pltpu.VMEM),
+        scratch_shapes=scratch,
+        compiler_params=pltpu.CompilerParams(
+            collective_id=0, has_side_effects=True, vmem_limit_bytes=60 * 2**20
+        ),
+        name="layer",
+    )(*args)
+
+
+def suits(mesh, sizes):
+    n, pair = mesh.shape["sp"], mesh.shape["tp"]
+    x_rows, queries, keys, gate = sizes
+    if pair != 2 or n % 2:
+        return False
+    rows, group = x_rows[0] // n, n // 2
+    heads = keys[1] // pair // HEAD_SIZE
+    units = gate[1] // pair
+    return (
+        rows % GRID_ROW_WIDTH == 0
+        and rows % 32 == 0
+        and queries[1] == 2 * keys[1]
+        and n % heads == 0
+        and 2 * HEAD_SIZE == LANES
+        and x_rows[1] == n * LANES
+        and units % (16 * group) == 0
+    )
+
 
 def solution(mesh):
     placed = (
@@ -201,6 +669,12 @@
         P(None, "tp"),
         P("sp", "tp"),
     )
-    return jax.shard_map(
-        shards, mesh=mesh, in_specs=placed, out_specs=P("sp", None), check_vma=False
-    )
+    def run(*arrays):
+        n = mesh.shape["sp"]
+        fits = suits(mesh, [arrays[k].shape for k in (0, 1, 2, 8)])
+        local = functools.partial(kernel_shards, n, 2) if fits else shards
+        return jax.shard_map(
+            local, mesh=mesh, in_specs=placed, out_specs=P("sp", None), check_vma=False
+        )(*arrays)
+
+    return run

time: 566 us -> 188 us (0.33)
  waiting for transfers between devices: 485 us -> 0 us
  Pallas kernels: 0 us -> 177 us
  matrix products: 33.7 us -> 0 us
  between operations: 13.8 us -> 0.1 us
  other arithmetic: 13.5 us -> 2.22 us
    all_gather x5 -> x0, waiting for transfers between devices: 461 us -> none  [the longest x1 128 us: shards(): lax.all_gather(value_weight, 'sp', axis=0, tiled=True)]
    pallas_call x0 -> x1, Pallas kernels: none -> 177 us  [kernel_shards(): pl.pallas_call(lambda *refs: layer_kernel(n, halves, *refs), out_shape=ja...]
    dot_general x6 -> x0, matrix products: 33.7 us -> none  [the longest x1 9.19 us: contract_units(): lax.dot_general(left_rows, right_rows, (((1,), (1,)), ((), ())), preferre...]
    reduce_scatter x2 -> x0, waiting for transfers between devices: 17.7 us -> none  [the longest x1 9.03 us: shards(): lax.psum_scatter(contract_units(hidden, collected[2]).astype(jnp.bfloat16...]
  transfers between devices with their start and end apart: 9 -> 0, of which waited for: 8 -> 0; matrix products, arithmetic and copies ran while one was open for 6% -> 0% of each run, Pallas kernels for 0% -> 0%
where the time goes in v1:
time: 188 us
  Pallas kernels  177 us (94%)
  local copies, waits for them, and re-layouts  8.83 us (5%)
  other arithmetic  2.22 us (1%)
    pallas_call x1, Pallas kernels, kernel_shards(): pl.pallas_call(lambda *refs: layer_kernel(n, halves, *refs), out_shape=ja...  177 us

profile of v1, /device:TPU:7, one launch (start us, length us, event | category | flops | bytes accessed | tf_op | source)
XLA Modules:
  0.0 188.2 jit_solution(18208005312788605768)
XLA Ops:
  0.0 0.0 copy-start
  0.0 1.5 constant_dynamic-slice_fusion
  1.5 0.8 sine_multiply_fusion
  2.2 1.4 copy.20
  3.6 1.4 copy.21
  5.1 0.0 copy-done
  5.1 0.3 copy.22
  5.4 0.0 copy-start.1
  5.4 0.0 copy-start.2
  5.4 0.0 copy-start.3
  5.4 0.0 copy-start.4
  5.4 1.4 pad_maximum_fusion.refs_9_
  6.9 0.0 copy-done.1
  6.9 0.1 copy.17
  7.0 0.0 copy-done.2
  7.0 0.1 copy.18
  7.1 0.8 copy.23.refs_2_
  7.9 0.0 copy-done.3
  7.9 0.7 broadcast_in_dim_tile.6.refs_3_
  8.6 0.0 copy-done.4
  8.6 0.7 broadcast_in_dim_tile.7.refs_4_
  9.3 177.1 %layer.1 = bf16[128,2048]{1,0:T(8,128)(2,1)} custom-call(bf16[128,2048]{1,0:T(8,128)(2,1)} %refs_0_.1, bf16[128,512]{1,0:T(8,128)(2,1)} %refs_1_.1, bf16[128,512]{1,0:T(8,128)(2,1)} %copy.23.refs_2_, f32[1,128]{1,0:T(1,128)} %broadcast_in_dim_tile.6.refs_3_, f32[1,128]{1,0:T(1,128)} %broadcast_in_dim_tile.7.refs_4_, f32[64,128]{1,0:T(8,128)} %get-tuple-element.6.refs_5_, ...), custom_call_target="tpu_custom_call" | custom-call | tf_op jit(solution)/shard_map/layer/pallas_call | solution.py:624
  186.3 1.9 copy.25
  (4 shorter events, 0.0 us)
Async XLA Ops:
  0.0 5.1 %copy-start = (bf16[128,2560]{1,0:T(8,128)(2,1)S(1)}, bf16[128,2560]{1,0:T(8,128)(2,1)}, u32[]{:S(2)}) copy-start(bf16[128,2560]{1,0:T(8,128)(2,1)} %param.25) | copy-start | bytes 1966084
  5.4 1.5 copy-start.1
  5.4 1.6 copy-start.2
  5.4 2.5 %copy-start.3 = (f32[64]{0:T(128)S(1)}, f32[64]{0:T(128)}, u32[]{:S(2)}) copy-start(f32[64]{0:T(128)} %param.17) | copy-start | bytes 772
  5.4 3.2 %copy-start.4 = (f32[64]{0:T(128)S(1)}, f32[64]{0:T(128)}, u32[]{:S(2)}) copy-start(f32[64]{0:T(128)} %param.18) | copy-start | bytes 772

commit v2 on v1

--- a/solution.py
+++ b/solution.py
@@ -193,17 +193,21 @@
 F32 = jnp.float32
 
 
+def rem(a, b):
+    return a % b if isinstance(a, int) else lax.rem(a, b)
+
+
 def nt(left, right):
     return lax.dot_general(left, right, (((1,), (1,)), ((), ())), preferred_element_type=F32)
 
 
 def layer_kernel(
-    n, halves, x_ref, q_ref, kv_ref, qg_ref, kg_ref, cos_ref, sin_ref, wo_ref, fg_ref, w_ref,
+    n, x_ref, q_ref, kv_ref, qg_ref, kg_ref, cos_ref, sin_ref, wo_ref, fg_ref, w_ref,
     cg_ref, cv_ref, out_ref,
-    kvbuf, qbuf, kcat, qcat, att_s, attbuf, po_s, po_r, mid, allnorm, halo_s, halo_r, wrecv,
+    kvbuf, qbuf, kcat, qcat, att_s, attbuf, po_s, po_r, mid, allnorm, edge_s, edge_r, wrecv,
     pre_g, pre_v, part, ddbuf, own_sum, rs_s, rs_r, fin_s, fin_r,
-    loc, kv_ss, kv_rs, q_ss, q_rs, w_ss, w_rs, o_ss, o_rs, po_sem, ag_ss, ag_rs, fw_ss, fw_rs,
-    h_ss, h_rs, dd_ss, dd_rs, c_ss, c_rs, fin_sem,
+    loc, kv_ss, kv_rs, q_ss, q_rs, w_ss, w_rs, wf_ss, wf_rs, dw_ss, dw_rs, df_ss, df_rs, o_ss, o_rs, po_sem, ag_ss, ag_rs, fw_ss, fw_rs,
+    h_sem, dd_ss, dd_rs, c_ss, c_rs, fin_sem,
 ):
     sp = lax.axis_index("sp")
     core = lax.axis_index("tp")
@@ -212,15 +216,30 @@
     half_rows = rows // 2
     width = x_ref.shape[1]
     kv_heads = kv_ref.shape[1] // LANES
-    group = n // halves
+    plane = n // 4
+    group = 2 * plane
     tokens = n * rows
     q_tokens = kv_heads * rows
     units = w_ref.shape[1] // 3
-    head_at = lax.rem(sp, kv_heads)
+    head_at = rem(sp, kv_heads)
     q_base = sp - head_at
-    in_group = lax.rem(sp, group)
-    g_base = sp - in_group
-    half_at = sp // group
+    place = rem(sp, plane)
+    side = rem(sp // plane, 2)
+    wing = sp // (2 * plane)
+    member = wing * plane + place
+
+    def chip(m, at_side):
+        return (m // plane) * (2 * plane) + at_side * plane + rem(m, plane)
+
+    def ahead(d):
+        return rem(wing + d // plane, 2) * plane + rem(place + rem(d, plane), plane)
+
+    def behind(d):
+        return rem(wing + d // plane, 2) * plane + rem(
+            place + plane - rem(d, plane), plane
+        )
+
+    twin = chip(member, 1 - side)
 
     def remote(src, dst, ss, rs, device):
         return pltpu.make_async_remote_copy(
@@ -243,7 +262,7 @@
     barrier = pltpu.get_barrier_semaphore()
 
     def greet(d):
-        t = lax.rem(sp + d, n)
+        t = rem(sp + d, n)
         pl.semaphore_signal(barrier, inc=1, device_id=(t, core), device_id_type=MESH)
         pl.semaphore_signal(barrier, inc=1, device_id=(t, mate), device_id_type=MESH)
 
@@ -252,25 +271,49 @@
     pl.semaphore_wait(barrier, 2 * n - 1)
 
     def q_copy(d):
-        t = q_base + lax.rem(head_at + d, kv_heads)
+        t = q_base + rem(head_at + d, kv_heads)
         return remote(
             q_ref.at[:, lane_block(t - q_base)], qbuf.at[span(head_at * rows, rows, rows)],
             q_ss.at[d], q_rs.at[d], (t, core),
         )
 
     def kv_copy(d):
-        t = lax.rem(sp + d, n)
+        t = rem(sp + d, n)
         return remote(
-            kv_ref.at[:, lane_block(lax.rem(t, kv_heads))], kvbuf.at[span(sp * rows, rows, rows)],
+            kv_ref.at[:, lane_block(rem(t, kv_heads))], kvbuf.at[span(sp * rows, rows, rows)],
             kv_ss.at[d], kv_rs.at[d], (t, core),
         )
 
-    def w_copy(d):
-        t = lax.rem(sp + d, n)
+    up_part, down_part = slice(0, 2 * units), slice(2 * units, 3 * units)
+
+    def w_copy(d, part_at, ss, rs):
+        m = ahead(d)
         return remote(
-            w_ref.at[lax.rem(t, group)], wrecv.at[:, lane_block(sp)],
-            w_ss.at[d], w_rs.at[d], (t, core),
-        )
+            w_ref.at[m, part_at], wrecv.at[part_at, lane_block(sp)],
+            ss.at[d], rs.at[d], (chip(m, side), core),
+        )
+
+    def twin_first(part_at, ss, rs):
+        return remote(
+            w_ref.at[member, part_at], wrecv.at[part_at, lane_block(sp)],
+            ss.at[0], rs.at[0], (twin, core),
+        )
+
+    def twin_copy(d, part_at, ss, rs):
+        at = wrecv.at[part_at, lane_block(chip(behind(d), side))]
+        return remote(at, at, ss.at[d], rs.at[d], (twin, core))
+
+    def pass_on(d, part_at, ss, rs, next_ss, next_rs):
+        dst = wrecv.at[part_at, lane_block(chip(behind(d), side))]
+        remote(dst, dst, ss.at[d], rs.at[d], (twin, core)).wait_recv()
+        twin_copy(d, part_at, next_ss, next_rs).start()
+
+    def twin_wait(d, part_at, ss, rs):
+        dst = wrecv.at[part_at, lane_block(chip(behind(d), 1 - side))]
+        remote(dst, dst, ss.at[d], rs.at[d], (twin, core)).wait_recv()
+
+    gate_sems, gate_next = (w_ss, w_rs), (wf_ss, wf_rs)
+    down_sems, down_next = (dw_ss, dw_rs), (df_ss, df_rs)
 
     own_q = pltpu.make_async_copy(
         q_ref.at[:, lane_block(head_at)], qbuf.at[span(head_at * rows, rows, rows)], loc.at[0]
@@ -278,18 +321,19 @@
     own_kv = pltpu.make_async_copy(
         kv_ref.at[:, lane_block(head_at)], kvbuf.at[span(sp * rows, rows, rows)], loc.at[1]
     )
-    own_w = pltpu.make_async_copy(w_ref.at[in_group], wrecv.at[:, lane_block(sp)], loc.at[2])
+    own_w = pltpu.make_async_copy(w_ref.at[member], wrecv.at[:, lane_block(sp)], loc.at[2])
     own_q.start()
     own_kv.start()
     loop(1, kv_heads, lambda d: q_copy(d).start())
     loop(1, n, lambda d: kv_copy(d).start())
-    loop(1, n, lambda d: w_copy(d).start())
+    loop(1, group, lambda d: w_copy(d, up_part, *gate_sems).start())
+    twin_first(up_part, *gate_next).start()
     own_w.start()
 
     lane = lax.broadcasted_iota(jnp.int32, (GRID_ROW_WIDTH, LANES), 1)
     low = lane < HEAD_SIZE
-    first = lax.rem(lane, 2 * HEAD_SIZE // 4) < HEAD_SIZE // 4
-    by_row = lax.rem(lane, HEAD_SIZE) < HEAD_SIZE // 2
+    first = rem(lane, 2 * HEAD_SIZE // 4) < HEAD_SIZE // 4
+    by_row = rem(lane, HEAD_SIZE) < HEAD_SIZE // 2
 
     def turn(vals, grid_row):
         cos = jnp.where(by_row, cos_ref[pl.ds(grid_row, 1), :], cos_ref[:GRID_ROW_WIDTH, :])
@@ -303,15 +347,6 @@
     def split(vals):
         top = vals.astype(BF).astype(F32)
         return top, (vals - top).astype(BF).astype(F32)
-
-    own_q.wait()
-
-    def q_wait(d):
-        s = lax.rem(head_at + kv_heads - d, kv_heads)
-        dst = qbuf.at[span(s * rows, rows, rows)]
-        remote(dst, dst, q_ss.at[d], q_rs.at[d], (q_base + s, core)).wait_recv()
-
-    loop(1, kv_heads, q_wait)
 
     def make_q(r):
         at = span(r * GRID_ROW_WIDTH, GRID_ROW_WIDTH, GRID_ROW_WIDTH)
@@ -330,15 +365,21 @@
         later = span(q_tokens + r * GRID_ROW_WIDTH, GRID_ROW_WIDTH, GRID_ROW_WIDTH)
         qcat[later, :] = jnp.where(low, pltpu.roll(top, HEAD_SIZE, 1), rest).astype(BF)
 
-    loop(0, q_tokens // GRID_ROW_WIDTH, make_q)
-    own_kv.wait()
-
-    def kv_wait(d):
-        s = lax.rem(sp + n - d, n)
-        dst = kvbuf.at[span(s * rows, rows, rows)]
-        remote(dst, dst, kv_ss.at[d], kv_rs.at[d], (s, core)).wait_recv()
-
-    loop(1, n, kv_wait)
+    own_q.wait()
+
+    def q_take(d):
+        s = rem(head_at + kv_heads - d, kv_heads)
+        dst = qbuf.at[span(s * rows, rows, rows)]
+
+        @pl.when(d > 0)
+        def _():
+            remote(dst, dst, q_ss.at[d], q_rs.at[d], (q_base + s, core)).wait_recv()
+
+        for r in range(rows // GRID_ROW_WIDTH):
+            make_q(s * (rows // GRID_ROW_WIDTH) + r)
+
+    loop(0, kv_heads, q_take)
+    steps = rows // GRID_ROW_WIDTH
 
     def make_k(r):
         at = span(r * GRID_ROW_WIDTH, GRID_ROW_WIDTH, GRID_ROW_WIDTH)
@@ -351,10 +392,24 @@
         kcat[at, :LANES] = jnp.where(low, top, pltpu.roll(top, HEAD_SIZE, 1)).astype(BF)
         kcat[at, LANES:] = jnp.where(low, rest, pltpu.roll(rest, HEAD_SIZE, 1)).astype(BF)
 
-    loop(0, tokens // GRID_ROW_WIDTH, make_k)
+    own_kv.wait()
+
+    def kv_take(d):
+        s = rem(sp + n - d, n)
+        dst = kvbuf.at[span(s * rows, rows, rows)]
+
+        @pl.when(d > 0)
+        def _():
+            remote(dst, dst, kv_ss.at[d], kv_rs.at[d], (s, core)).wait_recv()
+
+        for r in range(steps):
+            make_k(s * steps + r)
+
+    loop(0, n, kv_take)
+    loop(1, plane, lambda d: pass_on(d, up_part, *gate_sems, *gate_next))
 
     def o_copy(d):
-        k = lax.rem(head_at + d, kv_heads)
+        k = rem(head_at + d, kv_heads)
         return remote(
             att_s.at[span(k * rows, rows, rows)], attbuf.at[:, lane_block(head_at)],
             o_ss.at[d], o_rs.at[d], (q_base + k, core),
@@ -376,7 +431,7 @@
         ).astype(BF)
 
     def attend_send(d):
-        k = lax.rem(head_at + d, kv_heads)
+        k = rem(head_at + d, kv_heads)
         att_s[span(k * rows, rows, rows), :] = attend(k)
 
         @pl.when(d < kv_heads)
@@ -387,7 +442,7 @@
     attbuf[:, lane_block(head_at)] = att_s[span(head_at * rows, rows, rows), :]
 
     def o_wait(d):
-        s = lax.rem(head_at + kv_heads - d, kv_heads)
+        s = rem(head_at + kv_heads - d, kv_heads)
         dst = attbuf.at[:, lane_block(s)]
         remote(dst, dst, o_ss.at[d], o_rs.at[d], (q_base + s, core)).wait_recv()
 
@@ -410,95 +465,90 @@
     def slot(k, c):
         return allnorm.at[span(k * rows + c * half_rows, half_rows, half_rows)]
 
-    allnorm[span(in_group * rows + core * half_rows, half_rows, half_rows), :] = normed
-
-    wide = normed.astype(F32)
-    pieces = width // LANES
-
-    def halo_fill(row):
-        for k in range(pieces):
-            halo_s[k : k + 1, :] = wide[row : row + 1, k * LANES : (k + 1) * LANES]
-
-    def halo_copy(k):
-        other = (1 - half_at) * group
+    allnorm[span(member * rows + core * half_rows, half_rows, half_rows), :] = normed
+
+    def ag_copy(d):
+        to = ahead(rem(d, plane)) if d != plane else ahead(d)
+        of = member if d <= plane else (1 - wing) * plane + place
         return remote(
-            halo_s, halo_r, h_ss.at[k], h_rs.at[0], (other + k // 2, lax.rem(k, 2))
-        )
-
-    sends_first = jnp.logical_and(jnp.logical_and(half_at == 1, in_group == 0), core == 0)
-    sends_last = jnp.logical_and(jnp.logical_and(half_at == 0, in_group == group - 1), core == 1)
-
-    @pl.when(sends_first)
-    def _():
-        halo_fill(0)
-
-    @pl.when(sends_last)
-    def _():
-        halo_fill(half_rows - 1)
-
-    sends = jnp.logical_or(sends_first, sends_last)
-
-    @pl.when(sends)
-    def _():
-        loop(0, 2 * group, lambda k: halo_copy(k).start())
-
-    def ag_copy(d):
-        t = g_base + lax.rem(in_group + d, group)
-        return remote(
-            slot(in_group, core), slot(in_group, core), ag_ss.at[d], ag_rs.at[d], (t, core)
+            slot(of, core), slot(of, core), ag_ss.at[d], ag_rs.at[d], (chip(to, side), core)
         )
 
     def fw_copy(d):
-        s = lax.rem(in_group + group - d, group)
+        s = behind(d)
         return remote(slot(s, core), slot(s, core), fw_ss.at[d], fw_rs.at[d], (sp, mate))
 
-    loop(1, group, lambda d: ag_copy(d).start())
-    fw_copy(0).start()
-
     def ag_wait(d):
-        s = lax.rem(in_group + group - d, group)
+        s = behind(d)
         remote(slot(s, core), slot(s, core), ag_ss.at[d], ag_rs.at[d], (sp, mate)).wait_recv()
         fw_copy(d).start()
 
+    ag_copy(plane).start()
+    for d in range(1, plane):
+        ag_copy(d).start()
+    fw_copy(0).start()
+    loop(1, group, lambda d: w_copy(d, down_part, *down_sems).start())
+    twin_first(down_part, *down_next).start()
+
     own_w.wait()
-
-    def w_wait(d):
-        s = lax.rem(sp + n - d, n)
-        dst = wrecv.at[:, lane_block(s)]
-        remote(dst, dst, w_ss.at[d], w_rs.at[d], (s, core)).wait_recv()
-
-    loop(1, n, w_wait)
+    loop(plane, group, lambda d: pass_on(d, up_part, *gate_sems, *gate_next))
+    ag_wait(plane)
+    for d in range(plane + 1, group):
+        ag_copy(d).start()
+    loop(0, group, lambda d: twin_wait(d, up_part, *gate_next))
 
     def up(block):
         both = nt(block, wrecv[: 2 * units, :]).astype(BF).astype(F32)
         return both[:, :units], both[:, units:]
 
+    seg = plane * rows
+    pitch = seg + 16
+
+    def row_of(m):
+        return (m // plane) * pitch + rem(m, plane) * rows
+
     def up_rows(d):
-        s = lax.rem(in_group + group - d, group)
-
-        @pl.when(d > 0)
+        s = behind(d)
+
+        @pl.when(jnp.logical_and(d > 0, d != plane))
         def _():
             ag_wait(d)
 
         remote(slot(s, mate), slot(s, mate), fw_ss.at[d], fw_rs.at[d], (sp, mate)).wait_recv()
         gate, value = up(allnorm[span(s * rows, rows, rows), :])
-        at = span(8 + s * rows, rows, 8)
+        at = span(row_of(s) + 8, rows, 8)
         pre_g[at, :] = gate
         pre_v[at, :] = value
 
-    loop(0, group, up_rows)
-    remote(halo_r, halo_r, h_ss.at[0], h_rs.at[0], (sp, mate)).wait_recv()
-    edge = jnp.concatenate([halo_r[k : k + 1, :] for k in range(pieces)], axis=1)
-    gate, value = up(jnp.broadcast_to(edge, (16, width)).astype(BF))
-    span_rows = group * rows
-    zeros = jnp.zeros((8, units), F32)
-    pre_g[:8, :] = jnp.where(half_at == 1, gate[:8], zeros)
-    pre_v[:8, :] = jnp.where(half_at == 1, value[:8], zeros)
-    pre_g[8 + span_rows :, :] = jnp.where(half_at == 0, gate[:8], zeros)
-    pre_v[8 + span_rows :, :] = jnp.where(half_at == 0, value[:8], zeros)
+    loop(0, plane + 1, up_rows)
+    loop(1, group, lambda d: pass_on(d, down_part, *down_sems, *down_next))
+    loop(plane + 1, group, up_rows)
+
+    edge_at = (8, 8 + seg - 1, pitch + 8, pitch + 8 + seg - 1)
+    edge_s[...] = jnp.concatenate(
+        [
+            jnp.concatenate([pre[k : k + 1, :] for k in edge_at] * 2, axis=0)
+            for pre in (pre_g, pre_v)
+        ],
+        axis=0,
+    )
+    edge_copy = remote(edge_s, edge_r, h_sem.at[0], h_sem.at[1], (twin, core))
+    edge_copy.start()
+    loop(0, group, lambda d: twin_wait(d, down_part, *down_next))
+    edge_copy.wait_recv()
+    for pre, first_row in ((pre_g, 0), (pre_v, 8)):
+        near = [
+            jnp.broadcast_to(edge_r[first_row + k : first_row + k + 1, :], (8, units))
+            for k in range(4)
+        ]
+        none = jnp.zeros((8, units), F32)
+        pre[0:8, :] = jnp.where(side == 0, none, near[1])
+        pre[8 + seg : pitch, :] = jnp.where(side == 0, near[0], near[2])
+        pre[pitch : pitch + 8, :] = jnp.where(side == 0, near[1], near[3])
+        pre[pitch + 8 + seg :, :] = jnp.where(side == 0, near[2], none)
 
     def convolve(ref, taps, k):
-        block = ref[span(k * rows, rows + 16, 8), :]
+        block = ref[span(row_of(k), rows + 16, 8), :]
         return (
             taps[0:1, :] * block[7 : 7 + rows]
             + taps[1:2, :] * block[8 : 8 + rows]
@@ -511,9 +561,11 @@
             dd_ss.at[d], dd_rs.at[d], (sp, mate),
         )
 
-    def c_copy(d):
-        t = g_base + lax.rem(in_group + d, group)
-        return remote(rs_s.at[d], rs_r.at[d], c_ss.at[d], c_rs.at[d], (t, core))
+    def c_copy(d, to):
+        return remote(rs_s.at[d], rs_r.at[d], c_ss.at[d], c_rs.at[d], (chip(to, side), core))
+
+    def c_near(d):
+        return c_copy(d, ahead(rem(d, plane)))
 
     def combine(d):
         dd_copy(d).wait_recv()
@@ -521,29 +573,38 @@
 
     def send_sum(d):
         rs_s[d] = combine(d).astype(BF)
-        c_copy(d).start()
-
-    def down(d):
-        k = lax.rem(in_group + d, group)
+        c_near(d).start()
+
+    def order(j):
+        return plane * (1 - j // plane) + rem(j + 1, plane)
+
+    def down(j):
+        d = order(j)
+        k = ahead(d)
         gate = convolve(pre_g, cg_ref, k)
         value = convolve(pre_v, cv_ref, k)
         hidden = (gate / (1.0 + jnp.exp(-gate)) * value).astype(BF)
-        e = lax.rem(d, group)
-        part[e] = jnp.dot(hidden, wrecv[2 * units :, :], preferred_element_type=F32).astype(BF)
-        dd_copy(e).start()
-
-        @pl.when(d > 1)
+        part[d] = jnp.dot(hidden, wrecv[2 * units :, :], preferred_element_type=F32).astype(BF)
+        dd_copy(d).start()
+        last = order(jnp.maximum(j - 1, 0))
+
+        @pl.when(jnp.logical_and(j > 0, rem(last, plane) > 0))
         def _():
-            send_sum(d - 1)
-
-    loop(1, group + 1, down)
-    own_sum[...] = mid[...] + combine(0)
+            send_sum(last)
+
+    loop(0, group, down)
 
     def add_in(d):
         remote(rs_r.at[d], rs_r.at[d], c_ss.at[d], c_rs.at[d], (sp, mate)).wait_recv()
         own_sum[...] = own_sum[...] + rs_r[d].astype(F32)
 
-    loop(1, group, add_in)
+    own_sum[...] = combine(plane)
+    loop(plane + 1, group, add_in)
+    rs_s[plane] = own_sum[...].astype(BF)
+    far_copy = c_copy(plane, (1 - wing) * plane + place)
+    far_copy.start()
+    own_sum[...] = mid[...] + combine(0)
+    loop(1, plane + 1, add_in)
     fin_s[...] = own_sum[...].astype(BF)
     fin_copy = remote(fin_s, fin_r, fin_sem.at[0], fin_sem.at[1], (sp, mate))
     fin_copy.start()
@@ -551,18 +612,20 @@
 
     loop(1, kv_heads, lambda d: q_copy(d).wait_send())
     loop(1, n, lambda d: kv_copy(d).wait_send())
-    loop(1, n, lambda d: w_copy(d).wait_send())
+    loop(1, group, lambda d: w_copy(d, up_part, *gate_sems).wait_send())
+    loop(1, group, lambda d: w_copy(d, down_part, *down_sems).wait_send())
+    loop(0, group, lambda d: twin_copy(d, up_part, *gate_next).wait_send())
+    loop(0, group, lambda d: twin_copy(d, down_part, *down_next).wait_send())
     loop(1, kv_heads, lambda d: o_copy(d).wait_send())
     po_copy.wait_send()
-    loop(1, group, lambda d: ag_copy(d).wait_send())
+    for d in range(1, group):
+        ag_copy(d).wait_send()
     loop(0, group, lambda d: fw_copy(d).wait_send())
-
-    @pl.when(sends)
-    def _():
-        loop(0, 2 * group, lambda k: halo_copy(k).wait_send())
-
+    edge_copy.wait_send()
     loop(0, group, lambda d: dd_copy(d).wait_send())
-    loop(1, group, lambda d: c_copy(d).wait_send())
+    loop(1, plane, lambda d: c_near(d).wait_send())
+    loop(plane + 1, group, lambda d: c_near(d).wait_send())
+    far_copy.wait_send()
     fin_copy.wait_send()
     fin_copy.wait_recv()
     out_ref[span(mate * half_rows, half_rows, half_rows), :] = fin_r[...]
@@ -579,12 +642,13 @@
 
 
 def kernel_shards(
-    n, halves, x_rows, queries, keys, values, query_norm_gain, key_norm_gain, out_weight, ffn_gain,
+    n, x_rows, queries, keys, values, query_norm_gain, key_norm_gain, out_weight, ffn_gain,
     gate_weight, value_weight, conv_gate, conv_value, down_weight,
 ):
     rows, width = x_rows.shape
     kv_heads = keys.shape[1] // HEAD_SIZE
-    group = n // halves
+    plane = n // 4
+    group = 2 * plane
     unit_local = gate_weight.shape[1]
     units = unit_local // group
     depth = gate_weight.shape[0]
@@ -595,7 +659,8 @@
         w.T.reshape(group, units, depth) for w in (gate_weight, value_weight, down_weight)
     ]
     weights = jnp.concatenate(turned, axis=1)
-    chip = lax.rem(lax.axis_index("sp"), group)
+    at = lax.axis_index("sp")
+    chip = (at // group) * plane + rem(at, plane)
     taps = [lax.dynamic_slice_in_dim(t, chip * units, units, 1) for t in (conv_gate, conv_value)]
     cos, sin = rotary_tables(max(GRID_ROW_WIDTH, n * rows // GRID_ROW_WIDTH))
     tokens, q_tokens, span_rows = n * rows, kv_heads * rows, group * rows
@@ -606,15 +671,15 @@
         vm((tokens, LANES), BF), vm((q_tokens, LANES), BF), vm((tokens, 2 * LANES), BF),
         vm((2 * q_tokens, LANES), BF), vm((q_tokens, LANES), BF), vm((rows, kv_heads * LANES), BF),
         vm((rows, width), BF), vm((half_rows, width), BF), vm((half_rows, width), F32),
-        vm((span_rows, width), BF), vm((width // LANES, LANES), F32),
-        vm((width // LANES, LANES), F32), vm((3 * units, width), BF),
-        vm((span_rows + 16, units), F32), vm((span_rows + 16, units), F32),
+        vm((span_rows, width), BF), vm((16, units), F32),
+        vm((16, units), F32), vm((3 * units, width), BF),
+        vm((span_rows + 32, units), F32), vm((span_rows + 32, units), F32),
         vm((group, rows, width), BF), vm((group, half_rows, width), BF),
         vm((half_rows, width), F32), vm((group, half_rows, width), BF),
         vm((group, half_rows, width), BF), vm((half_rows, width), BF), vm((half_rows, width), BF),
-        dma((3,)), dma((n,)), dma((n,)), dma((kv_heads,)), dma((kv_heads,)), dma((n,)), dma((n,)),
+        dma((3,)), dma((n,)), dma((n,)), dma((kv_heads,)), dma((kv_heads,)), *[dma((group,))] * 8,
         dma((kv_heads,)), dma((kv_heads,)), dma((2,)), dma((group,)), dma((group,)),
-        dma((group,)), dma((group,)), dma((2 * group,)), dma((1,)), dma((group,)), dma((group,)),
+        dma((group,)), dma((group,)), dma((2,)), dma((group,)), dma((group,)),
         dma((group,)), dma((group,)), dma((2,)),
     ]
     args = (
@@ -622,7 +687,7 @@
         cos, sin, out_weight, ffn_gain[None, :], weights, taps[0], taps[1],
     )
     return pl.pallas_call(
-        lambda *refs: layer_kernel(n, halves, *refs),
+        lambda *refs: layer_kernel(n, *refs),
         out_shape=jax.ShapeDtypeStruct((rows, width), BF),
         in_specs=[pl.BlockSpec(memory_space=pltpu.VMEM)] * len(args),
         out_specs=pl.BlockSpec(memory_space=pltpu.VMEM),
@@ -637,7 +702,7 @@
 def suits(mesh, sizes):
     n, pair = mesh.shape["sp"], mesh.shape["tp"]
     x_rows, queries, keys, gate = sizes
-    if pair != 2 or n % 2:
+    if pair != 2 or n % 4:
         return False
     rows, group = x_rows[0] // n, n // 2
     heads = keys[1] // pair // HEAD_SIZE
@@ -672,7 +737,7 @@
     def run(*arrays):
         n = mesh.shape["sp"]
         fits = suits(mesh, [arrays[k].shape for k in (0, 1, 2, 8)])
-        local = functools.partial(kernel_shards, n, 2) if fits else shards
+        local = functools.partial(kernel_shards, n) if fits else shards
         return jax.shard_map(
             local, mesh=mesh, in_specs=placed, out_specs=P("sp", None), check_vma=False
         )(*arrays)

time: 188 us -> 153 us (0.81)
  the two profiles are of different devices: /device:TPU:7 before, /device:TPU:9 now
where the time goes in v2:
time: 153 us
  Pallas kernels  142 us (93%)
  local copies, waits for them, and re-layouts  8.83 us (6%)
  other arithmetic  2.22 us (1%)
    pallas_call x1, Pallas kernels, kernel_shards(): pl.pallas_call(lambda *refs: layer_kernel(n, *refs), out_shape=jax.ShapeD...  142 us
    transpose x3, local copies, waits for them, and re-layouts, kernel_shards(): w.T.reshape(group, units, depth)  3.14 us

profile of v2, /device:TPU:9, one launch (start us, length us, event | category | flops | bytes accessed | tf_op | source)
XLA Modules:
  0.0 153.0 jit_solution(7174767556397559396)
XLA Ops:
  0.0 0.0 copy-start
  0.0 1.5 constant_dynamic-slice_fusion
  1.5 0.8 sine_multiply_fusion
  2.2 1.4 copy.20
  3.6 1.4 copy.21
  5.1 0.0 copy-done
  5.1 0.3 copy.22
  5.4 0.0 copy-start.1
  5.4 0.0 copy-start.2
  5.4 0.0 copy-start.3
  5.4 0.0 copy-start.4
  5.4 1.4 pad_maximum_fusion.refs_9_
  6.9 0.0 copy-done.1
  6.9 0.1 copy.17
  7.0 0.0 copy-done.2
  7.0 0.1 copy.18
  7.1 0.8 copy.23.refs_2_
  7.9 0.0 copy-done.3
  7.9 0.7 broadcast_in_dim_tile.6.refs_3_
  8.6 0.0 copy-done.4
  8.6 0.7 broadcast_in_dim_tile.7.refs_4_
  9.3 141.9 %layer.1 = bf16[128,2048]{1,0:T(8,128)(2,1)} custom-call(bf16[128,2048]{1,0:T(8,128)(2,1)} %refs_0_.1, bf16[128,512]{1,0:T(8,128)(2,1)} %refs_1_.1, bf16[128,512]{1,0:T(8,128)(2,1)} %copy.23.refs_2_, f32[1,128]{1,0:T(1,128)} %broadcast_in_dim_tile.6.refs_3_, f32[1,128]{1,0:T(1,128)} %broadcast_in_dim_tile.7.refs_4_, f32[64,128]{1,0:T(8,128)} %get-tuple-element.6.refs_5_, ...), custom_call_target="tpu_custom_call" | custom-call | tf_op jit(solution)/shard_map/layer/pallas_call | solution.py:689
  151.2 1.9 %copy.25 = bf16[128,2048]{1,0:T(8,128)(2,1)} copy(bf16[128,2048]{1,0:T(8,128)(2,1)} %layer.1) | data formatting | bytes 1048576
  (4 shorter events, 0.0 us)
Async XLA Ops:
  0.0 5.1 %copy-start = (bf16[128,2560]{1,0:T(8,128)(2,1)S(1)}, bf16[128,2560]{1,0:T(8,128)(2,1)}, u32[]{:S(2)}) copy-start(bf16[128,2560]{1,0:T(8,128)(2,1)} %param.25) | copy-start | bytes 1966084
  5.4 1.5 copy-start.1
  5.4 1.6 %copy-start.2 = (bf16[128,256]{1,0:T(8,128)(2,1)S(1)}, bf16[128,256]{1,0:T(8,128)(2,1)}, u32[]{:S(2)}) copy-start(bf16[128,256]{1,0:T(8,128)(2,1)} %param.16) | copy-start | bytes 196612
  5.4 2.5 %copy-start.3 = (f32[64]{0:T(128)S(1)}, f32[64]{0:T(128)}, u32[]{:S(2)}) copy-start(f32[64]{0:T(128)} %param.17) | copy-start | bytes 772
  5.4 3.2 %copy-start.4 = (f32[64]{0:T(128)S(1)}, f32[64]{0:T(128)}, u32[]{:S(2)}) copy-start(f32[64]{0:T(128)} %param.18) | copy-start | bytes 772

commit v3 on v2

--- a/solution.py
+++ b/solution.py
@@ -204,7 +204,7 @@
 def layer_kernel(
     n, x_ref, q_ref, kv_ref, qg_ref, kg_ref, cos_ref, sin_ref, wo_ref, fg_ref, w_ref,
     cg_ref, cv_ref, out_ref,
-    kvbuf, qbuf, kcat, qcat, att_s, attbuf, po_s, po_r, mid, allnorm, edge_s, edge_r, wrecv,
+    wo_buf, kvbuf, qbuf, kcat, qcat, att_s, attbuf, po_s, po_r, mid, allnorm, edge_s, edge_r, wrecv,
     pre_g, pre_v, part, ddbuf, own_sum, rs_s, rs_r, fin_s, fin_r,
     loc, kv_ss, kv_rs, q_ss, q_rs, w_ss, w_rs, wf_ss, wf_rs, dw_ss, dw_rs, df_ss, df_rs, o_ss, o_rs, po_sem, ag_ss, ag_rs, fw_ss, fw_rs,
     h_sem, dd_ss, dd_rs, c_ss, c_rs, fin_sem,
@@ -264,11 +264,10 @@
     def greet(d):
         t = rem(sp + d, n)
         pl.semaphore_signal(barrier, inc=1, device_id=(t, core), device_id_type=MESH)
-        pl.semaphore_signal(barrier, inc=1, device_id=(t, mate), device_id_type=MESH)
 
     loop(1, n, greet)
     pl.semaphore_signal(barrier, inc=1, device_id=(sp, mate), device_id_type=MESH)
-    pl.semaphore_wait(barrier, 2 * n - 1)
+    pl.semaphore_wait(barrier, n)
 
     def q_copy(d):
         t = q_base + rem(head_at + d, kv_heads)
@@ -312,6 +311,7 @@
         dst = wrecv.at[part_at, lane_block(chip(behind(d), 1 - side))]
         remote(dst, dst, ss.at[d], rs.at[d], (twin, core)).wait_recv()
 
+    later = plane + plane // 2
     gate_sems, gate_next = (w_ss, w_rs), (wf_ss, wf_rs)
     down_sems, down_next = (dw_ss, dw_rs), (df_ss, df_rs)
 
@@ -323,11 +323,12 @@
     )
     own_w = pltpu.make_async_copy(w_ref.at[member], wrecv.at[:, lane_block(sp)], loc.at[2])
     own_q.start()
+    wo_copy = pltpu.make_async_copy(wo_ref, wo_buf, loc.at[3])
+    wo_copy.start()
     own_kv.start()
     loop(1, kv_heads, lambda d: q_copy(d).start())
     loop(1, n, lambda d: kv_copy(d).start())
-    loop(1, group, lambda d: w_copy(d, up_part, *gate_sems).start())
-    twin_first(up_part, *gate_next).start()
+    loop(1, plane, lambda d: w_copy(d, up_part, *gate_sems).start())
     own_w.start()
 
     lane = lax.broadcasted_iota(jnp.int32, (GRID_ROW_WIDTH, LANES), 1)
@@ -343,6 +344,9 @@
             first, pltpu.roll(vals, LANES - quarter, 1), pltpu.roll(vals, quarter, 1)
         )
         return vals * cos + swapped * sin
+
+    q_gain = jnp.concatenate([qg_ref[...]] * 2, axis=1)
+    k_gain = jnp.concatenate([kg_ref[...]] * 2, axis=1)
 
     def split(vals):
         top = vals.astype(BF).astype(F32)
@@ -359,7 +363,7 @@
             lax.rsqrt(low_sum * (1.0 / HEAD_SIZE) + eps_norm),
             lax.rsqrt(high_sum * (1.0 / HEAD_SIZE) + eps_norm),
         )
-        turned = turn(vals * inverse * qg_ref[...], q_base * (rows // GRID_ROW_WIDTH) + r)
+        turned = turn(vals * inverse * q_gain, q_base * (rows // GRID_ROW_WIDTH) + r)
         top, rest = split(turned * HEAD_SIZE ** (-0.5))
         qcat[at, :] = jnp.where(low, top, pltpu.roll(rest, HEAD_SIZE, 1)).astype(BF)
         later = span(q_tokens + r * GRID_ROW_WIDTH, GRID_ROW_WIDTH, GRID_ROW_WIDTH)
@@ -379,6 +383,8 @@
             make_q(s * (rows // GRID_ROW_WIDTH) + r)
 
     loop(0, kv_heads, q_take)
+    twin_first(up_part, *gate_next).start()
+    loop(plane, later, lambda d: w_copy(d, up_part, *gate_sems).start())
     steps = rows // GRID_ROW_WIDTH
 
     def make_k(r):
@@ -386,7 +392,7 @@
         vals = kvbuf[at, :].astype(F32)
         total = jnp.sum(jnp.where(low, vals * vals, 0.0), axis=1, keepdims=True)
         turned = turn(
-            vals * lax.rsqrt(total * (1.0 / HEAD_SIZE) + eps_norm) * kg_ref[...], r
+            vals * lax.rsqrt(total * (1.0 / HEAD_SIZE) + eps_norm) * k_gain, r
         )
         top, rest = split(turned)
         kcat[at, :LANES] = jnp.where(low, top, pltpu.roll(top, HEAD_SIZE, 1)).astype(BF)
@@ -448,7 +454,8 @@
 
     loop(1, kv_heads, o_wait)
 
-    po_s[...] = jnp.dot(attbuf[...], wo_ref[...], preferred_element_type=F32).astype(BF)
+    wo_copy.wait()
+    po_s[...] = jnp.dot(attbuf[...], wo_buf[...], preferred_element_type=F32).astype(BF)
     po_copy = remote(
         po_s.at[span(mate * half_rows, half_rows, half_rows)], po_r, po_sem.at[0], po_sem.at[1],
         (sp, mate),
@@ -487,15 +494,17 @@
     for d in range(1, plane):
         ag_copy(d).start()
     fw_copy(0).start()
-    loop(1, group, lambda d: w_copy(d, down_part, *down_sems).start())
-    twin_first(down_part, *down_next).start()
 
     own_w.wait()
-    loop(plane, group, lambda d: pass_on(d, up_part, *gate_sems, *gate_next))
+    loop(later, group, lambda d: w_copy(d, up_part, *gate_sems).start())
+    loop(plane, later, lambda d: pass_on(d, up_part, *gate_sems, *gate_next))
     ag_wait(plane)
     for d in range(plane + 1, group):
         ag_copy(d).start()
-    loop(0, group, lambda d: twin_wait(d, up_part, *gate_next))
+    loop(plane, group, lambda d: w_copy(d, down_part, *down_sems).start())
+    loop(1, plane, lambda d: w_copy(d, down_part, *down_sems).start())
+    loop(later, group, lambda d: pass_on(d, up_part, *gate_sems, *gate_next))
+    twin_first(down_part, *down_next).start()
 
     def up(block):
         both = nt(block, wrecv[: 2 * units, :]).astype(BF).astype(F32)
@@ -507,22 +516,27 @@
     def row_of(m):
         return (m // plane) * pitch + rem(m, plane) * rows
 
-    def up_rows(d):
-        s = behind(d)
-
+    def take(d):
         @pl.when(jnp.logical_and(d > 0, d != plane))
         def _():
             ag_wait(d)
 
+    def mate_wait(d):
+        s = behind(d)
         remote(slot(s, mate), slot(s, mate), fw_ss.at[d], fw_rs.at[d], (sp, mate)).wait_recv()
-        gate, value = up(allnorm[span(s * rows, rows, rows), :])
-        at = span(row_of(s) + 8, rows, 8)
+
+    def up_rows(k):
+        side_at = rem(wing + k, 2)
+        loop(k * plane, (k + 1) * plane, mate_wait)
+        gate, value = up(allnorm[span(side_at * seg, seg, rows), :])
+        at = span(side_at * pitch + 8, seg, 8)
         pre_g[at, :] = gate
         pre_v[at, :] = value
 
-    loop(0, plane + 1, up_rows)
+    loop(0, group, take)
+    loop(0, group, lambda d: twin_wait(d, up_part, *gate_next))
+    loop(0, 2, up_rows)
     loop(1, group, lambda d: pass_on(d, down_part, *down_sems, *down_next))
-    loop(plane + 1, group, up_rows)
 
     edge_at = (8, 8 + seg - 1, pitch + 8, pitch + 8 + seg - 1)
     edge_s[...] = jnp.concatenate(
@@ -668,7 +682,7 @@
     dma = pltpu.SemaphoreType.DMA
     vm = pltpu.VMEM
     scratch = [
-        vm((tokens, LANES), BF), vm((q_tokens, LANES), BF), vm((tokens, 2 * LANES), BF),
+        vm(out_weight.shape, BF), vm((tokens, LANES), BF), vm((q_tokens, LANES), BF), vm((tokens, 2 * LANES), BF),
         vm((2 * q_tokens, LANES), BF), vm((q_tokens, LANES), BF), vm((rows, kv_heads * LANES), BF),
         vm((rows, width), BF), vm((half_rows, width), BF), vm((half_rows, width), F32),
         vm((span_rows, width), BF), vm((16, units), F32),
@@ -677,19 +691,21 @@
         vm((group, rows, width), BF), vm((group, half_rows, width), BF),
         vm((half_rows, width), F32), vm((group, half_rows, width), BF),
         vm((group, half_rows, width), BF), vm((half_rows, width), BF), vm((half_rows, width), BF),
-        dma((3,)), dma((n,)), dma((n,)), dma((kv_heads,)), dma((kv_heads,)), *[dma((group,))] * 8,
+        dma((4,)), dma((n,)), dma((n,)), dma((kv_heads,)), dma((kv_heads,)), *[dma((group,))] * 8,
         dma((kv_heads,)), dma((kv_heads,)), dma((2,)), dma((group,)), dma((group,)),
         dma((group,)), dma((group,)), dma((2,)), dma((group,)), dma((group,)),
         dma((group,)), dma((group,)), dma((2,)),
     ]
     args = (
-        x_rows, queries, kv, jnp.tile(query_norm_gain, 2)[None, :], jnp.tile(key_norm_gain, 2)[None, :],
+        x_rows, queries, kv, query_norm_gain[None, :], key_norm_gain[None, :],
         cos, sin, out_weight, ffn_gain[None, :], weights, taps[0], taps[1],
     )
     return pl.pallas_call(
         lambda *refs: layer_kernel(n, *refs),
         out_shape=jax.ShapeDtypeStruct((rows, width), BF),
-        in_specs=[pl.BlockSpec(memory_space=pltpu.VMEM)] * len(args),
+        in_specs=[
+            pl.BlockSpec(memory_space=pl.ANY if a is out_weight else pltpu.VMEM) for a in args
+        ],
         out_specs=pl.BlockSpec(memory_space=pltpu.VMEM),
         scratch_shapes=scratch,
         compiler_params=pltpu.CompilerParams(

time: 153 us -> 136 us (0.89)
  the two profiles are of different devices: /device:TPU:9 before, /device:TPU:7 now
where the time goes in v3:
time: 136 us; the launch traced here: 135 us
  Pallas kernels  125 us (92%)
  local copies, waits for them, and re-layouts  7.48 us (6%)
  other arithmetic  2.22 us (2%)
    pallas_call x1, Pallas kernels, kernel_shards(): pl.pallas_call(lambda *refs: layer_kernel(n, *refs), out_shape=jax.ShapeD...  125 us
    transpose x3, local copies, waits for them, and re-layouts, kernel_shards(): w.T.reshape(group, units, depth)  3.14 us

profile of v3, /device:TPU:7, one launch (start us, length us, event | category | flops | bytes accessed | tf_op | source)
XLA Modules:
  0.0 134.8 jit_solution(18295970786862416626)
XLA Ops:
  0.0 0.0 copy-start
  0.0 1.4 %constant_dynamic-slice_fusion = (f32[3,320]{1,0:T(4,128)}, f32[3,320]{1,0:T(4,128)}) fusion(f32[3,2560]{1,0:T(4,128)} %param.24, s32[]{:T(128)S(6)} %select_n.41, f32[3,2560]{1,0:T(4,128)} %param.23), kind=kLoop, calls=%fused_computation.12 | loop fusion | bytes 15364 | tf_op jit(solution)/shard_map/dynamic_slice | solution.py:678
  1.5 0.8 sine_multiply_fusion
  2.2 1.4 %copy.22 = bf16[2560,128]{1,0:T(8,128)(2,1)S(1)} copy(bf16[2560,128]{0,1:T(8,128)(2,1)} %bitcast.15) | data formatting | bytes 1310720 | tf_op jit(solution)/shard_map/transpose | solution.py:673
  3.6 1.4 %copy.20 = bf16[2560,128]{1,0:T(8,128)(2,1)S(1)} copy(bf16[2560,128]{0,1:T(8,128)(2,1)} %bitcast.16) | data formatting | bytes 1310720 | tf_op jit(solution)/shard_map/transpose | solution.py:673
  5.1 0.0 copy-done
  5.1 0.3 copy.21
  5.4 0.0 copy-start.1
  5.4 0.0 copy-start.2
  5.4 1.4 %pad_maximum_fusion.refs_9_ = bf16[8,960,128]{2,1,0:T(8,128)(2,1)} fusion(bf16[8,320,128]{2,1,0:T(8,128)(2,1)S(1)} %bitcast.12, bf16[8,320,128]{2,1,0:T(8,128)(2,1)S(1)} %bitcast.14, bf16[8,320,128]{2,1,0:T(8,128)(2,1)S(1)} %bitcast.13), kind=kLoop, calls=%fused_computation | loop fusion | flops 5898240 | bytes 3932160 | tf_op jit(solution)/shard_map/concatenate | solution.py:675
  6.9 0.0 copy-done.1
  6.9 0.1 copy.17
  7.0 0.0 copy-done.2
  7.0 0.1 copy.18
  7.1 0.8 copy.23.refs_2_
  7.9 125.0 %layer.1 = bf16[128,2048]{1,0:T(8,128)(2,1)} custom-call(bf16[128,2048]{1,0:T(8,128)(2,1)} %refs_0_.1, bf16[128,512]{1,0:T(8,128)(2,1)} %refs_1_.1, bf16[128,512]{1,0:T(8,128)(2,1)} %copy.23.refs_2_, f32[1,64]{1,0:T(1,128)} %bitcast.22, f32[1,64]{1,0:T(1,128)} %bitcast.23, f32[64,128]{1,0:T(8,128)} %get-tuple-element.6.refs_5_, ...), custom_call_target="tpu_custom_call" | custom-call | tf_op jit(solution)/shard_map/layer/pallas_call | solution.py:703
  132.9 1.9 %copy.25 = bf16[128,2048]{1,0:T(8,128)(2,1)} copy(bf16[128,2048]{1,0:T(8,128)(2,1)} %layer.1) | data formatting | bytes 1048576
  (2 shorter events, 0.0 us)
Async XLA Ops:
  0.0 5.1 %copy-start = (bf16[128,2560]{1,0:T(8,128)(2,1)S(1)}, bf16[128,2560]{1,0:T(8,128)(2,1)}, u32[]{:S(2)}) copy-start(bf16[128,2560]{1,0:T(8,128)(2,1)} %param.22) | copy-start | bytes 1966084
  5.4 1.5 %copy-start.1 = (bf16[128,256]{1,0:T(8,128)(2,1)S(1)}, bf16[128,256]{1,0:T(8,128)(2,1)}, u32[]{:S(2)}) copy-start(bf16[128,256]{1,0:T(8,128)(2,1)} %param.15) | copy-start | bytes 196612
  5.4 1.6 %copy-start.2 = (bf16[128,256]{1,0:T(8,128)(2,1)S(1)}, bf16[128,256]{1,0:T(8,128)(2,1)}, u32[]{:S(2)}) copy-start(bf16[128,256]{1,0:T(8,128)(2,1)} %param.16) | copy-start | bytes 196612

commit v4 on v3

--- a/solution.py
+++ b/solution.py
@@ -207,7 +207,7 @@
     wo_buf, kvbuf, qbuf, kcat, qcat, att_s, attbuf, po_s, po_r, mid, allnorm, edge_s, edge_r, wrecv,
     pre_g, pre_v, part, ddbuf, own_sum, rs_s, rs_r, fin_s, fin_r,
     loc, kv_ss, kv_rs, q_ss, q_rs, w_ss, w_rs, wf_ss, wf_rs, dw_ss, dw_rs, df_ss, df_rs, o_ss, o_rs, po_sem, ag_ss, ag_rs, fw_ss, fw_rs,
-    h_sem, dd_ss, dd_rs, c_ss, c_rs, fin_sem,
+    ch_ss, ch_rs, h_sem, dd_ss, dd_rs, c_ss, c_rs, fin_sem,
 ):
     sp = lax.axis_index("sp")
     core = lax.axis_index("tp")
@@ -329,6 +329,7 @@
     loop(1, kv_heads, lambda d: q_copy(d).start())
     loop(1, n, lambda d: kv_copy(d).start())
     loop(1, plane, lambda d: w_copy(d, up_part, *gate_sems).start())
+    loop(1, plane, lambda d: w_copy(d, down_part, *down_sems).start())
     own_w.start()
 
     lane = lax.broadcasted_iota(jnp.int32, (GRID_ROW_WIDTH, LANES), 1)
@@ -497,14 +498,14 @@
 
     own_w.wait()
     loop(later, group, lambda d: w_copy(d, up_part, *gate_sems).start())
+    twin_first(down_part, *down_next).start()
+    loop(1, plane, lambda d: pass_on(d, down_part, *down_sems, *down_next))
     loop(plane, later, lambda d: pass_on(d, up_part, *gate_sems, *gate_next))
     ag_wait(plane)
     for d in range(plane + 1, group):
         ag_copy(d).start()
     loop(plane, group, lambda d: w_copy(d, down_part, *down_sems).start())
-    loop(1, plane, lambda d: w_copy(d, down_part, *down_sems).start())
     loop(later, group, lambda d: pass_on(d, up_part, *gate_sems, *gate_next))
-    twin_first(down_part, *down_next).start()
 
     def up(block):
         both = nt(block, wrecv[: 2 * units, :]).astype(BF).astype(F32)
@@ -535,8 +536,8 @@
 
     loop(0, group, take)
     loop(0, group, lambda d: twin_wait(d, up_part, *gate_next))
+    loop(plane, group, lambda d: pass_on(d, down_part, *down_sems, *down_next))
     loop(0, 2, up_rows)
-    loop(1, group, lambda d: pass_on(d, down_part, *down_sems, *down_next))
 
     edge_at = (8, 8 + seg - 1, pitch + 8, pitch + 8 + seg - 1)
     edge_s[...] = jnp.concatenate(
@@ -581,13 +582,32 @@
     def c_near(d):
         return c_copy(d, ahead(rem(d, plane)))
 
+    quarter_rows = half_rows // 2
+
+    def c_half(d, h, to):
+        at = span(h * quarter_rows, quarter_rows, quarter_rows)
+        return remote(
+            rs_s.at[d, at], rs_r.at[d, at], ch_ss.at[2 * d + h], ch_rs.at[2 * d + h],
+            (chip(to, side), core),
+        )
+
+    def c_cross(d, h):
+        return c_half(d, h, ahead(rem(d, plane)))
+
     def combine(d):
         dd_copy(d).wait_recv()
         return part[d, mine, :].astype(F32) + ddbuf[d].astype(F32)
 
     def send_sum(d):
         rs_s[d] = combine(d).astype(BF)
-        c_near(d).start()
+
+        @pl.when(d < plane)
+        def _():
+            c_near(d).start()
+
+        @pl.when(d > plane)
+        def _():
+            c_cross(d, 0).start()
 
     def order(j):
         return plane * (1 - j // plane) + rem(j + 1, plane)
@@ -606,6 +626,10 @@
         def _():
             send_sum(last)
 
+        @pl.when(j == plane)
+        def _():
+            loop(plane + 1, group, lambda k: c_cross(k, 1).start())
+
     loop(0, group, down)
 
     def add_in(d):
@@ -613,12 +637,29 @@
         own_sum[...] = own_sum[...] + rs_r[d].astype(F32)
 
     own_sum[...] = combine(plane)
-    loop(plane + 1, group, add_in)
-    rs_s[plane] = own_sum[...].astype(BF)
-    far_copy = c_copy(plane, (1 - wing) * plane + place)
-    far_copy.start()
+    far = (1 - wing) * plane + place
+
+    def far_send(h):
+        at = span(h * quarter_rows, quarter_rows, quarter_rows)
+
+        def half_in(d):
+            c_cross(d, h).wait_recv()
+            own_sum[at, :] = own_sum[at, :] + rs_r[d, at, :].astype(F32)
+
+        loop(plane + 1, group, half_in)
+        rs_s[plane, at, :] = own_sum[at, :].astype(BF)
+        c_half(plane, h, far).start()
+
+    loop(0, 2, far_send)
     own_sum[...] = mid[...] + combine(0)
-    loop(1, plane + 1, add_in)
+    loop(1, plane, add_in)
+
+    def far_take(h):
+        at = span(h * quarter_rows, quarter_rows, quarter_rows)
+        c_half(plane, h, far).wait_recv()
+        own_sum[at, :] = own_sum[at, :] + rs_r[plane, at, :].astype(F32)
+
+    loop(0, 2, far_take)
     fin_s[...] = own_sum[...].astype(BF)
     fin_copy = remote(fin_s, fin_r, fin_sem.at[0], fin_sem.at[1], (sp, mate))
     fin_copy.start()
@@ -638,8 +679,10 @@
     edge_copy.wait_send()
     loop(0, group, lambda d: dd_copy(d).wait_send())
     loop(1, plane, lambda d: c_near(d).wait_send())
-    loop(plane + 1, group, lambda d: c_near(d).wait_send())
-    far_copy.wait_send()
+    for h in range(2):
+        for d in range(plane + 1, group):
+            c_cross(d, h).wait_send()
+        c_half(plane, h, far).wait_send()
     fin_copy.wait_send()
     fin_copy.wait_recv()
     out_ref[span(mate * half_rows, half_rows, half_rows), :] = fin_r[...]
@@ -693,7 +736,8 @@
         vm((group, half_rows, width), BF), vm((half_rows, width), BF), vm((half_rows, width), BF),
         dma((4,)), dma((n,)), dma((n,)), dma((kv_heads,)), dma((kv_heads,)), *[dma((group,))] * 8,
         dma((kv_heads,)), dma((kv_heads,)), dma((2,)), dma((group,)), dma((group,)),
-        dma((group,)), dma((group,)), dma((2,)), dma((group,)), dma((group,)),
+        dma((group,)), dma((group,)), dma((2 * group,)), dma((2 * group,)), dma((2,)),
+        dma((group,)), dma((group,)),
         dma((group,)), dma((group,)), dma((2,)),
     ]
     args = (

time: 136 us -> 130 us (0.956)
  Pallas kernels: 125 us -> 120 us
    pallas_call x1, Pallas kernels: 125 us -> 120 us  [kernel_shards(): pl.pallas_call(lambda *refs: layer_kernel(n, *refs), out_shape=jax.ShapeD...]
where the time goes in v4:
time: 130 us
  Pallas kernels  120 us (92%)
  local copies, waits for them, and re-layouts  7.48 us (6%)
  other arithmetic  2.22 us (2%)
    pallas_call x1, Pallas kernels, kernel_shards(): pl.pallas_call(lambda *refs: layer_kernel(n, *refs), out_shape=jax.ShapeD...  120 us
    transpose x3, local copies, waits for them, and re-layouts, kernel_shards(): w.T.reshape(group, units, depth)  3.14 us

profile of v4, /device:TPU:7, one launch (start us, length us, event | category | flops | bytes accessed | tf_op | source)
XLA Modules:
  0.0 129.6 jit_solution(2392821076573165866)
XLA Ops:
  0.0 0.0 copy-start
  0.0 1.4 %constant_dynamic-slice_fusion = (f32[3,320]{1,0:T(4,128)}, f32[3,320]{1,0:T(4,128)}) fusion(f32[3,2560]{1,0:T(4,128)} %param.24, s32[]{:T(128)S(6)} %select_n.41, f32[3,2560]{1,0:T(4,128)} %param.23), kind=kLoop, calls=%fused_computation.12 | loop fusion | bytes 15364 | tf_op jit(solution)/shard_map/dynamic_slice | solution.py:721
  1.5 0.8 sine_multiply_fusion
  2.2 1.4 %copy.22 = bf16[2560,128]{1,0:T(8,128)(2,1)S(1)} copy(bf16[2560,128]{0,1:T(8,128)(2,1)} %bitcast.15) | data formatting | bytes 1310720 | tf_op jit(solution)/shard_map/transpose | solution.py:716
  3.6 1.4 %copy.20 = bf16[2560,128]{1,0:T(8,128)(2,1)S(1)} copy(bf16[2560,128]{0,1:T(8,128)(2,1)} %bitcast.16) | data formatting | bytes 1310720 | tf_op jit(solution)/shard_map/transpose | solution.py:716
  5.1 0.0 copy-done
  5.1 0.3 copy.21
  5.4 0.0 copy-start.1
  5.4 0.0 copy-start.2
  5.4 1.4 %pad_maximum_fusion.refs_9_ = bf16[8,960,128]{2,1,0:T(8,128)(2,1)} fusion(bf16[8,320,128]{2,1,0:T(8,128)(2,1)S(1)} %bitcast.12, bf16[8,320,128]{2,1,0:T(8,128)(2,1)S(1)} %bitcast.14, bf16[8,320,128]{2,1,0:T(8,128)(2,1)S(1)} %bitcast.13), kind=kLoop, calls=%fused_computation | loop fusion | flops 5898240 | bytes 3932160 | tf_op jit(solution)/shard_map/concatenate | solution.py:718
  6.9 0.0 copy-done.1
  6.9 0.1 copy.17
  7.0 0.0 copy-done.2
  7.0 0.1 copy.18
  7.1 0.8 copy.23.refs_2_
  7.9 119.9 %layer.1 = bf16[128,2048]{1,0:T(8,128)(2,1)} custom-call(bf16[128,2048]{1,0:T(8,128)(2,1)} %refs_0_.1, bf16[128,512]{1,0:T(8,128)(2,1)} %refs_1_.1, bf16[128,512]{1,0:T(8,128)(2,1)} %copy.23.refs_2_, f32[1,64]{1,0:T(1,128)} %bitcast.22, f32[1,64]{1,0:T(1,128)} %bitcast.23, f32[64,128]{1,0:T(8,128)} %get-tuple-element.6.refs_5_, ...), custom_call_target="tpu_custom_call" | custom-call | tf_op jit(solution)/shard_map/layer/pallas_call | solution.py:747
  127.7 1.9 %copy.25 = bf16[128,2048]{1,0:T(8,128)(2,1)} copy(bf16[128,2048]{1,0:T(8,128)(2,1)} %layer.1) | data formatting | bytes 1048576
  (2 shorter events, 0.0 us)
Async XLA Ops:
  0.0 5.1 %copy-start = (bf16[128,2560]{1,0:T(8,128)(2,1)S(1)}, bf16[128,2560]{1,0:T(8,128)(2,1)}, u32[]{:S(2)}) copy-start(bf16[128,2560]{1,0:T(8,128)(2,1)} %param.22) | copy-start | bytes 1966084
  5.4 1.5 %copy-start.1 = (bf16[128,256]{1,0:T(8,128)(2,1)S(1)}, bf16[128,256]{1,0:T(8,128)(2,1)}, u32[]{:S(2)}) copy-start(bf16[128,256]{1,0:T(8,128)(2,1)} %param.15) | copy-start | bytes 196612
  5.4 1.6 %copy-start.2 = (bf16[128,256]{1,0:T(8,128)(2,1)S(1)}, bf16[128,256]{1,0:T(8,128)(2,1)}, u32[]{:S(2)}) copy-start(bf16[128,256]{1,0:T(8,128)(2,1)} %param.16) | copy-start | bytes 196612

commit v5 on v4

--- a/solution.py
+++ b/solution.py
@@ -202,11 +202,11 @@
 
 
 def layer_kernel(
-    n, x_ref, q_ref, kv_ref, qg_ref, kg_ref, cos_ref, sin_ref, wo_ref, fg_ref, w_ref,
+    n, x_ref, q_ref, kv_ref, qg_ref, kg_ref, cos_ref, sin_ref, wo_ref, fg_ref, wg_ref, wv_ref, wd_ref,
     cg_ref, cv_ref, out_ref,
     wo_buf, kvbuf, qbuf, kcat, qcat, att_s, attbuf, po_s, po_r, mid, allnorm, edge_s, edge_r, wrecv,
     pre_g, pre_v, part, ddbuf, own_sum, rs_s, rs_r, fin_s, fin_r,
-    loc, kv_ss, kv_rs, q_ss, q_rs, w_ss, w_rs, wf_ss, wf_rs, dw_ss, dw_rs, df_ss, df_rs, o_ss, o_rs, po_sem, ag_ss, ag_rs, fw_ss, fw_rs,
+    loc, kv_ss, kv_rs, q_ss, q_rs, w_ss, w_rs, wv_ss, wv_rs, wf_ss, wf_rs, dw_ss, dw_rs, df_ss, df_rs, o_ss, o_rs, po_sem, ag_ss, ag_rs, fw_ss, fw_rs,
     ch_ss, ch_rs, h_sem, dd_ss, dd_rs, c_ss, c_rs, fin_sem,
 ):
     sp = lax.axis_index("sp")
@@ -220,7 +220,7 @@
     group = 2 * plane
     tokens = n * rows
     q_tokens = kv_heads * rows
-    units = w_ref.shape[1] // 3
+    units = wd_ref.shape[1]
     head_at = rem(sp, kv_heads)
     q_base = sp - head_at
     place = rem(sp, plane)
@@ -285,35 +285,59 @@
 
     up_part, down_part = slice(0, 2 * units), slice(2 * units, 3 * units)
 
-    def w_copy(d, part_at, ss, rs):
+    gate_part, value_part = slice(0, units), slice(units, 2 * units)
+
+    def w_copy(d, src, part_at, ss, rs):
         m = ahead(d)
         return remote(
-            w_ref.at[m, part_at], wrecv.at[part_at, lane_block(sp)],
-            ss.at[d], rs.at[d], (chip(m, side), core),
-        )
-
-    def twin_first(part_at, ss, rs):
-        return remote(
-            w_ref.at[member, part_at], wrecv.at[part_at, lane_block(sp)],
-            ss.at[0], rs.at[0], (twin, core),
+            src.at[m], wrecv.at[part_at, lane_block(sp)], ss.at[d], rs.at[d], (chip(m, side), core)
+        )
+
+    def w_copies(d):
+        return (
+            w_copy(d, wg_ref, gate_part, w_ss, w_rs),
+            w_copy(d, wv_ref, value_part, wv_ss, wv_rs),
+            w_copy(d, wd_ref, down_part, dw_ss, dw_rs),
+        )
+
+    def up_send(d):
+        for one in w_copies(d)[:2]:
+            one.start()
+
+    def down_send(d):
+        w_copies(d)[2].start()
+
+    own_parts = ((wg_ref, gate_part), (wv_ref, value_part), (wd_ref, down_part))
+
+    def own_copy(k):
+        src, part_at = own_parts[k]
+        return pltpu.make_async_copy(
+            src.at[member], wrecv.at[part_at, lane_block(sp)], loc.at[(2, 4, 5)[k]]
         )
 
     def twin_copy(d, part_at, ss, rs):
         at = wrecv.at[part_at, lane_block(chip(behind(d), side))]
         return remote(at, at, ss.at[d], rs.at[d], (twin, core))
 
-    def pass_on(d, part_at, ss, rs, next_ss, next_rs):
+    def land(d, part_at, rs):
         dst = wrecv.at[part_at, lane_block(chip(behind(d), side))]
-        remote(dst, dst, ss.at[d], rs.at[d], (twin, core)).wait_recv()
-        twin_copy(d, part_at, next_ss, next_rs).start()
+        remote(dst, dst, w_ss.at[d], rs.at[d], (twin, core)).wait_recv()
+
+    def up_pass(d):
+        land(d, gate_part, w_rs)
+        land(d, value_part, wv_rs)
+        twin_copy(d, up_part, *gate_next).start()
+
+    def down_pass(d):
+        land(d, down_part, dw_rs)
+        twin_copy(d, down_part, *down_next).start()
 
     def twin_wait(d, part_at, ss, rs):
         dst = wrecv.at[part_at, lane_block(chip(behind(d), 1 - side))]
         remote(dst, dst, ss.at[d], rs.at[d], (twin, core)).wait_recv()
 
     later = plane + plane // 2
-    gate_sems, gate_next = (w_ss, w_rs), (wf_ss, wf_rs)
-    down_sems, down_next = (dw_ss, dw_rs), (df_ss, df_rs)
+    gate_next, down_next = (wf_ss, wf_rs), (df_ss, df_rs)
 
     own_q = pltpu.make_async_copy(
         q_ref.at[:, lane_block(head_at)], qbuf.at[span(head_at * rows, rows, rows)], loc.at[0]
@@ -321,16 +345,16 @@
     own_kv = pltpu.make_async_copy(
         kv_ref.at[:, lane_block(head_at)], kvbuf.at[span(sp * rows, rows, rows)], loc.at[1]
     )
-    own_w = pltpu.make_async_copy(w_ref.at[member], wrecv.at[:, lane_block(sp)], loc.at[2])
     own_q.start()
     wo_copy = pltpu.make_async_copy(wo_ref, wo_buf, loc.at[3])
     wo_copy.start()
     own_kv.start()
     loop(1, kv_heads, lambda d: q_copy(d).start())
     loop(1, n, lambda d: kv_copy(d).start())
-    loop(1, plane, lambda d: w_copy(d, up_part, *gate_sems).start())
-    loop(1, plane, lambda d: w_copy(d, down_part, *down_sems).start())
-    own_w.start()
+    loop(1, plane, up_send)
+    loop(1, plane, down_send)
+    for k in range(3):
+        own_copy(k).start()
 
     lane = lax.broadcasted_iota(jnp.int32, (GRID_ROW_WIDTH, LANES), 1)
     low = lane < HEAD_SIZE
@@ -384,8 +408,10 @@
             make_q(s * (rows // GRID_ROW_WIDTH) + r)
 
     loop(0, kv_heads, q_take)
-    twin_first(up_part, *gate_next).start()
-    loop(plane, later, lambda d: w_copy(d, up_part, *gate_sems).start())
+    for k in range(3):
+        own_copy(k).wait()
+    twin_copy(0, up_part, *gate_next).start()
+    loop(plane, later, up_send)
     steps = rows // GRID_ROW_WIDTH
 
     def make_k(r):
@@ -413,7 +439,7 @@
             make_k(s * steps + r)
 
     loop(0, n, kv_take)
-    loop(1, plane, lambda d: pass_on(d, up_part, *gate_sems, *gate_next))
+    loop(1, plane, up_pass)
 
     def o_copy(d):
         k = rem(head_at + d, kv_heads)
@@ -496,16 +522,15 @@
         ag_copy(d).start()
     fw_copy(0).start()
 
-    own_w.wait()
-    loop(later, group, lambda d: w_copy(d, up_part, *gate_sems).start())
-    twin_first(down_part, *down_next).start()
-    loop(1, plane, lambda d: pass_on(d, down_part, *down_sems, *down_next))
-    loop(plane, later, lambda d: pass_on(d, up_part, *gate_sems, *gate_next))
+    loop(later, group, up_send)
+    twin_copy(0, down_part, *down_next).start()
+    loop(1, plane, down_pass)
+    loop(plane, later, up_pass)
     ag_wait(plane)
     for d in range(plane + 1, group):
         ag_copy(d).start()
-    loop(plane, group, lambda d: w_copy(d, down_part, *down_sems).start())
-    loop(later, group, lambda d: pass_on(d, up_part, *gate_sems, *gate_next))
+    loop(plane, group, down_send)
+    loop(later, group, up_pass)
 
     def up(block):
         both = nt(block, wrecv[: 2 * units, :]).astype(BF).astype(F32)
@@ -536,7 +561,7 @@
 
     loop(0, group, take)
     loop(0, group, lambda d: twin_wait(d, up_part, *gate_next))
-    loop(plane, group, lambda d: pass_on(d, down_part, *down_sems, *down_next))
+    loop(plane, group, down_pass)
     loop(0, 2, up_rows)
 
     edge_at = (8, 8 + seg - 1, pitch + 8, pitch + 8 + seg - 1)
@@ -667,8 +692,12 @@
 
     loop(1, kv_heads, lambda d: q_copy(d).wait_send())
     loop(1, n, lambda d: kv_copy(d).wait_send())
-    loop(1, group, lambda d: w_copy(d, up_part, *gate_sems).wait_send())
-    loop(1, group, lambda d: w_copy(d, down_part, *down_sems).wait_send())
+
+    def w_sent(d):
+        for one in w_copies(d):
+            one.wait_send()
+
+    loop(1, group, w_sent)
     loop(0, group, lambda d: twin_copy(d, up_part, *gate_next).wait_send())
     loop(0, group, lambda d: twin_copy(d, down_part, *down_next).wait_send())
     loop(1, kv_heads, lambda d: o_copy(d).wait_send())
@@ -715,7 +744,6 @@
     turned = [
         w.T.reshape(group, units, depth) for w in (gate_weight, value_weight, down_weight)
     ]
-    weights = jnp.concatenate(turned, axis=1)
     at = lax.axis_index("sp")
     chip = (at // group) * plane + rem(at, plane)
     taps = [lax.dynamic_slice_in_dim(t, chip * units, units, 1) for t in (conv_gate, conv_value)]
@@ -734,7 +762,7 @@
         vm((group, rows, width), BF), vm((group, half_rows, width), BF),
         vm((half_rows, width), F32), vm((group, half_rows, width), BF),
         vm((group, half_rows, width), BF), vm((half_rows, width), BF), vm((half_rows, width), BF),
-        dma((4,)), dma((n,)), dma((n,)), dma((kv_heads,)), dma((kv_heads,)), *[dma((group,))] * 8,
+        dma((6,)), dma((n,)), dma((n,)), dma((kv_heads,)), dma((kv_heads,)), *[dma((group,))] * 10,
         dma((kv_heads,)), dma((kv_heads,)), dma((2,)), dma((group,)), dma((group,)),
         dma((group,)), dma((group,)), dma((2 * group,)), dma((2 * group,)), dma((2,)),
         dma((group,)), dma((group,)),
@@ -742,7 +770,7 @@
     ]
     args = (
         x_rows, queries, kv, query_norm_gain[None, :], key_norm_gain[None, :],
-        cos, sin, out_weight, ffn_gain[None, :], weights, taps[0], taps[1],
+        cos, sin, out_weight, ffn_gain[None, :], *turned, taps[0], taps[1],
     )
     return pl.pallas_call(
         lambda *refs: layer_kernel(n, *refs),

time: 130 us -> 132 us (1.015)
  local copies, waits for them, and re-layouts: 7.48 us -> 10.4 us
  other arithmetic: 2.22 us -> 0.79 us
    unnamed x9 -> x7, local copies, waits for them, and re-layouts: 2.12 us -> 3.79 us
    concatenate x1 -> x0, other arithmetic: 1.43 us -> none  [kernel_shards(): weights = jnp.concatenate(turned, axis=1)]
where the time goes in v5:
time: 132 us; the launch traced here: 131 us
  Pallas kernels  120 us (91%)
  local copies, waits for them, and re-layouts  10.4 us (8%)
    pallas_call x1, Pallas kernels, kernel_shards(): pl.pallas_call(lambda *refs: layer_kernel(n, *refs), out_shape=jax.ShapeD...  120 us
    transpose x3, local copies, waits for them, and re-layouts, kernel_shards(): w.T.reshape(group, units, depth)  4.34 us
    unnamed x7, local copies, waits for them, and re-layouts  3.79 us

profile of v5, /device:TPU:7, one launch (start us, length us, event | category | flops | bytes accessed | tf_op | source)
XLA Modules:
  0.0 131.1 jit_solution(16544019319005826011)
XLA Ops:
  0.0 0.0 copy-start.1
  0.0 0.0 copy-start
  0.0 1.5 %constant_dynamic-slice_fusion = (f32[3,320]{1,0:T(4,128)}, f32[3,320]{1,0:T(4,128)}) fusion(f32[3,2560]{1,0:T(4,128)} %param.24, s32[]{:T(128)S(6)} %select_n.41, f32[3,2560]{1,0:T(4,128)} %param.23), kind=kLoop, calls=%fused_computation.11 | loop fusion | bytes 15364 | tf_op jit(solution)/shard_map/dynamic_slice | solution.py:749
  1.5 0.8 sine_multiply_fusion
  2.3 0.9 copy.17
  3.2 1.0 copy.18
  4.2 0.8 copy.23.refs_2_
  5.0 2.2 %copy.20 = bf16[2560,128]{1,0:T(8,128)(2,1)} copy(bf16[2560,128]{0,1:T(8,128)(2,1)} %bitcast.15) | data formatting | bytes 1310720 | tf_op jit(solution)/shard_map/transpose | solution.py:745
  7.2 0.0 copy-done
  7.2 1.1 copy.21
  8.2 0.0 copy-done.1
  8.2 1.1 copy.22
  9.3 119.9 %layer.1 = bf16[128,2048]{1,0:T(8,128)(2,1)} custom-call(bf16[128,2048]{1,0:T(8,128)(2,1)} %refs_0_.1, bf16[128,512]{1,0:T(8,128)(2,1)} %refs_1_.1, bf16[128,512]{1,0:T(8,128)(2,1)} %copy.23.refs_2_, f32[1,64]{1,0:T(1,128)} %bitcast.22, f32[1,64]{1,0:T(1,128)} %bitcast.23, f32[64,128]{1,0:T(8,128)} %get-tuple-element.6.refs_5_, ...), custom_call_target="tpu_custom_call" | custom-call | tf_op jit(solution)/shard_map/layer/pallas_call | solution.py:775
  129.3 1.9 %copy.25 = bf16[128,2048]{1,0:T(8,128)(2,1)} copy(bf16[128,2048]{1,0:T(8,128)(2,1)} %layer.1) | data formatting | bytes 1048576
  (2 shorter events, 0.0 us)
Async XLA Ops:
  0.0 8.2 %copy-start.1 = (bf16[128,2560]{1,0:T(8,128)(2,1)S(1)}, bf16[128,2560]{1,0:T(8,128)(2,1)}, u32[]{:S(2)}) copy-start(bf16[128,2560]{1,0:T(8,128)(2,1)} %param.25) | copy-start | bytes 1966084
  0.0 7.2 %copy-start = (bf16[128,2560]{1,0:T(8,128)(2,1)S(1)}, bf16[128,2560]{1,0:T(8,128)(2,1)}, u32[]{:S(2)}) copy-start(bf16[128,2560]{1,0:T(8,128)(2,1)} %param.22) | copy-start | bytes 1966084
